TPU v7x, 32 devices: a whole 2x2x4 slice. The times are simulated.
32 devices in a mesh: st: 16 (over z, y, x), tp: 2 (over core).
Axes of the slice: x: 2, y: 2, z: 4, core: 2. Of those that a mesh axis runs over, the one named last changes fastest.
Arguments:
- hidden: bfloat16 [16384, 2048], P('st'), may hold values from -6 to 6
- norm_gain: float32 [2048], replicated, may hold values from 0.1 to 1.9
- store: bfloat16 [384, 64, 2048], P('st'), may hold values from -6 to 6
- store_gain: float32 [2048], replicated, may hold values from 0.1 to 1.9
- passage_ids: int32 [128, 4], P('st'), may hold values from 0 to 383, as said below
- w_pool: bfloat16 [2048, 1024], P(None, 'tp'), may hold values from -0.125 to 0.125
- pool_mix: bfloat16 [4, 256, 256], P('tp'), may hold values from -0.375 to 0.375
- w_branch: bfloat16 [1024, 2048], P('tp'), may hold values from -0.1875 to 0.1875
- w_query: bfloat16 [2048, 512], P(None, 'tp'), may hold values from -0.125 to 0.125
- w_key: bfloat16 [2048, 512], P(None, 'tp'), may hold values from -0.125 to 0.125
- w_value: bfloat16 [2048, 512], P(None, 'tp'), may hold values from -0.125 to 0.125
- sharpness: float32 [4], P('tp'), may hold values from 1 to 90
- w_out: bfloat16 [512, 2048], P('tp'), may hold values from -0.25 to 0.25
- w_gate: bfloat16 [2048, 2048], P(None, 'tp'), may hold values from -0.125 to 0.125
Outputs:
- mixed: bfloat16 [16384, 2048], P('st', 'tp')
Inputs may be any that keep to these rules, and one draw needn't show every extreme that they name: `passage_ids`: passage p lies on index p // 24 of st. The ids of one sequence's blocks (aligned rows of 32 ids) name passages of at most 4 reads on any one holder, counted with repeats, and some sequence reaches 4 at some holder in every draw.
All inputs are finite; a program needn't handle non-finite values.
Results may differ from a plain program's by a relative error of at most 0.0095.
The roundings to bfloat16 on the way count: a program that leaves them out, or rounds other values in their place, can miss the bound.
Values may be sent and summed in bfloat16 or wider, within the bound.
A program may use at most 128 MiB of HBM per device.

v0:
```python
import functools
import math

import jax
import jax.numpy as jnp
from jax import lax
from jax.experimental import pallas as pl
from jax.experimental.pallas import tpu as pltpu
from jax.sharding import PartitionSpec as P

GROUPS = 4


def rms_norm(values, gain):
    wide = values.astype(jnp.float32)
    scale = lax.rsqrt(jnp.mean(wide * wide, axis=-1, keepdims=True) + 1e-05)
    return wide * scale * gain


def pool_branch(normed, w_pool, pool_mix):
    tokens = normed.shape[0]
    local_groups = pool_mix.shape[0]
    group_dim = pool_mix.shape[1]
    pool_in = jnp.dot(normed, w_pool, preferred_element_type=jnp.float32).astype(jnp.bfloat16)
    grouped = pool_in.astype(jnp.float32).reshape(tokens, local_groups, group_dim)
    group_index = lax.axis_index("tp") * local_groups + jnp.arange(local_groups, dtype=jnp.int32)
    window = jnp.power(2, group_index + 1)
    total = jnp.zeros_like(grouped)
    for shift in range(2**GROUPS):
        shifted = jnp.pad(grouped, ((shift, 0), (0, 0), (0, 0)))[:tokens]
        total = total + jnp.where(shift < window, 1.0, 0.0)[None, :, None] * shifted
    position = jnp.arange(tokens, dtype=jnp.int32)[:, None]
    count = jnp.minimum(position + 1, window[None, :]).astype(jnp.float32)
    pooled = (total / count[:, :, None] - grouped).astype(jnp.bfloat16)
    pool_out = jnp.einsum("tgc,gcd->tgd", pooled, pool_mix, preferred_element_type=jnp.float32)
    return pool_out.astype(jnp.bfloat16).reshape(tokens, local_groups * group_dim)


def half_terms(own, other, weight_own, weight_other):
    terms = [
        jnp.dot(a, w, preferred_element_type=jnp.float32).astype(jnp.bfloat16).astype(jnp.float32)
        for a, w in ((own, weight_own), (other, weight_other))
    ]
    return terms[0] + terms[1]


def swap(array):
    return lax.ppermute(array, "tp", [(0, 1), (1, 0)])


def columns_of(weight, part):
    half = weight.shape[1] // 2
    return lax.dynamic_slice_in_dim(weight, part * half, half, axis=1)


def attention_kernel(heads, slots_ref, scale_ref, q_ref, *refs):
    parts, out_ref = refs[:-1], refs[-1]
    kv = jnp.concatenate([r[0] for r in parts], axis=0)
    width = q_ref.shape[1]
    head_dim = width // heads
    for h in range(heads):
        cut = slice(h * head_dim, (h + 1) * head_dim)
        scores = lax.dot_general(
            q_ref[:, cut], kv[:, cut], (((1,), (1,)), ((), ())), preferred_element_type=jnp.float32
        )
        scores = scores * scale_ref[h]
        top = jnp.exp(scores - jnp.max(scores, axis=-1, keepdims=True))
        weights = (top / jnp.sum(top, axis=-1, keepdims=True)).astype(jnp.bfloat16)
        out_ref[:, cut] = jnp.dot(
            weights, kv[:, width + h * head_dim : width + (h + 1) * head_dim],
            preferred_element_type=jnp.float32,
        ).astype(jnp.bfloat16)


def attend(query, kv, block_slot, scale):
    blocks_dev, per_block = block_slot.shape
    tokens, width = query.shape
    block_len = tokens // blocks_dev
    length, both = kv.shape[1:]
    heads = scale.shape[0]

    def part(j):
        return pl.BlockSpec((1, length, both), lambda b, slots: (slots[b * per_block + j], 0, 0))

    return pl.pallas_call(
        functools.partial(attention_kernel, heads),
        out_shape=jax.ShapeDtypeStruct((tokens, width), jnp.bfloat16),
        grid_spec=pltpu.PrefetchScalarGridSpec(
            num_scalar_prefetch=1,
            grid=(blocks_dev,),
            in_specs=[
                pl.BlockSpec(memory_space=pltpu.SMEM),
                pl.BlockSpec((block_len, width), lambda b, slots: (b, 0)),
            ] + [part(j) for j in range(per_block)],
            out_specs=pl.BlockSpec((block_len, width), lambda b, slots: (b, 0)),
        ),
        cost_estimate=pl.CostEstimate(
            flops=4 * tokens * per_block * length * width, bytes_accessed=4 * 2**20, transcendentals=0
        ),
    )(block_slot.reshape(-1), scale, query, *([kv] * per_block))


def body(
    hidden,
    norm_gain,
    store,
    store_gain,
    passage_ids,
    w_pool,
    pool_mix,
    w_branch,
    w_query,
    w_key,
    w_value,
    sharpness,
    w_out,
    w_gate,
):
    holders = lax.axis_size("st")
    core = lax.axis_index("tp")
    flat_ids = passage_ids.reshape(-1)
    reads = flat_ids.shape[0]
    pass_dev, length, width = store.shape
    owner = flat_ids // pass_dev
    local = flat_ids % pass_dev
    order = jnp.arange(reads, dtype=jnp.int32)
    earlier = (owner[None, :] == owner[:, None]) & (order[None, :] < order[:, None])
    rank = jnp.sum(earlier.astype(jnp.int32), axis=1)
    most = max(1, 2 * reads // holders)
    wanted = owner * most + rank
    hits = wanted[None, :] == jnp.arange(holders * most, dtype=jnp.int32)[:, None]
    request = jnp.sum(jnp.where(hits, local[None, :], 0), axis=1).reshape(holders, most)
    incoming = lax.all_to_all(request, "st", split_axis=0, concat_axis=0, tiled=True)

    passage_normed = rms_norm(store, store_gain).astype(jnp.bfloat16).reshape(pass_dev * length, width)
    w_kv = jnp.concatenate([w_key, w_value], axis=1)
    own_kv = jnp.dot(passage_normed, w_kv, preferred_element_type=jnp.float32).astype(jnp.bfloat16)
    own_kv = own_kv.reshape(pass_dev, length, -1)
    packed = own_kv[incoming.reshape(-1)]
    packed, hidden, w_out, w_branch = lax.optimization_barrier((packed, hidden, w_out, w_branch))
    kv = lax.all_to_all(packed, "st", split_axis=0, concat_axis=0, tiled=True)
    slot = wanted

    w_out_other = swap(columns_of(w_out, 1 - core))
    w_branch_other = swap(columns_of(w_branch, 1 - core))
    normed = rms_norm(hidden, norm_gain).astype(jnp.bfloat16)
    pool_out = pool_branch(normed, w_pool, pool_mix)
    branch_pool = half_terms(pool_out, swap(pool_out), columns_of(w_branch, core), w_branch_other)
    gate = jax.nn.sigmoid(jnp.dot(normed, w_gate, preferred_element_type=jnp.float32))
    query = jnp.dot(normed, w_query, preferred_element_type=jnp.float32).astype(jnp.bfloat16)

    head_dim = query.shape[1] // sharpness.shape[0]
    read = attend(query, kv, slot.reshape(passage_ids.shape), sharpness / math.sqrt(head_dim))
    branch_read = half_terms(read, swap(read), columns_of(w_out, core), w_out_other)
    return (branch_pool + gate * branch_read).astype(jnp.bfloat16)


def solution(mesh):
    placed = (
        P("st", None),
        P(),
        P("st", None, None),
        P(),
        P("st", None),
        P(None, "tp"),
        P("tp", None, None),
        P("tp", None),
        P(None, "tp"),
        P(None, "tp"),
        P(None, "tp"),
        P("tp"),
        P("tp", None),
        P(None, "tp"),
    )
    return jax.shard_map(body, mesh=mesh, in_specs=placed, out_specs=P("st", "tp"), check_vma=False)
```

profile of v0, /device:TPU:15, one launch (start us, length us, event | category | flops | bytes accessed | tf_op | source)
XLA Modules:
  0.0 145.6 jit_solution(1937379162756912040)
XLA Ops:
  0.0 0.8 sign_compare_fusion
  0.8 0.7 broadcast_divide_fusion
  1.5 0.1 copy.79
  1.6 0.1 ne.399
  1.7 0.1 copy.81
  1.8 0.1 div.49
  1.9 0.1 copy.80
  2.0 0.1 rem.33
  2.1 0.2 convert_reduce_fusion
  2.3 0.1 select_reduce_fusion
  2.4 0.7 all_to_all.9
  3.0 6.6 %all-to-all-start = ((s32[16,1,4]{2,1,0:T(1,128)}), s32[16,1,4]{2,1,0:T(1,128)S(1)}, u32[]{:S(2)}, u32[]{:S(2)}) async-start(s32[16,1,4]{2,1,0:T(1,128)} %bitcast.2), calls=%async_computation | async-start | bytes 16384 | tf_op jit(solution)/shard_map/all_to_all | solution.py:133
  9.6 0.0 copy-start.7
  9.6 4.2 %fusion = f32[24,64]{1,0:T(8,128)S(1)} fusion(bf16[24,64,2048]{2,1,0:T(8,128)(2,1)} %param.16), kind=kLoop, calls=%fused_computation.3 | loop fusion | flops 9435648 | bytes 6297600 | tf_op jit(solution)/shard_map/reduce_sum | solution.py:16
  13.9 0.3 copy-done.1
  14.2 1.5 %fusion.2 = bf16[24,64,2048]{2,1,0:T(8,128)(2,1)S(1)} fusion(bf16[24,64,2048]{2,1,0:T(8,128)(2,1)S(1)} %copy-done.1, f32[2048]{0:T(1024)S(1)} %copy-done.7, f32[24,64]{1,0:T(8,128)S(1)} %add_rsqrt_fusion), kind=kLoop, calls=%fused_computation.5 | loop fusion | flops 12582912 | bytes 12597248 | tf_op jit(solution)/shard_map/convert_element_type | solution.py:135
  15.7 0.0 copy-done.11
  15.8 4.8 %convolution_convert_fusion = bf16[1536,512]{1,0:T(8,128)(2,1)} fusion(bf16[1536,2048]{1,0:T(8,128)(2,1)S(1)} %bitcast.22, bf16[2048,256]{1,0:T(8,128)(2,1)S(1)} %copy-done.10, bf16[2048,256]{1,0:T(8,128)(2,1)S(1)} %copy-done.11), kind=kOutput, calls=%fused_computation.12 | convolution fusion | flops 3226206208 | bytes 9961472 | tf_op jit(solution)/shard_map/dot_general | solution.py:137
  20.5 0.5 broadcast.2065
  21.1 0.6 reduce.3
  21.7 0.1 reshape.292
  21.8 4.2 %gather_fusion = bf16[64,64,512]{2,1,0:T(8,128)(2,1)} fusion(bf16[24,64,512]{2,1,0:T(8,128)(2,1)} %bitcast.21, s32[1024]{0:T(1024)S(1)} %pad_clamp_fusion), kind=kCustom, calls=%fused_computation | custom fusion | bytes 8388864 | tf_op jit(solution)/shard_map/gather | solution.py:139
  26.0 6.5 %all-to-all-start.1 = ((bf16[64,64,512]{2,1,0:T(8,128)(2,1)}), bf16[64,64,512]{2,1,0:T(8,128)(2,1)}, u32[]{:S(2)}, u32[]{:S(2)}) async-start(bf16[64,64,512]{2,1,0:T(8,128)(2,1)} %gather_fusion), calls=%async_computation.1 | async-start | bytes 8388608 | tf_op jit(solution)/shard_map/all_to_all | solution.py:141
  32.7 0.5 broadcast_multiply_fusion.scale_ref
  33.2 0.1 minimum_convert_fusion
  33.3 0.8 constant_dynamic-slice_fusion
  34.1 1.8 %collective-permute-start.3 = (bf16[256,1024]{1,0:T(8,128)(2,1)}, bf16[256,1024]{1,0:T(8,128)(2,1)}, u32[]{:S(2)}, u32[]{:S(2)}) collective-permute-start(bf16[256,1024]{1,0:T(8,128)(2,1)} %constant_dynamic-slice_fusion), channel_id=1, source_target_pairs={{0,1},{1,0},{2,3},{3,2},{4,5},{5,4},{6,7},{7,6},{8,9},{9,8},{10,11... | collective-permute-start | bytes 1572872 | tf_op jit(solution)/shard_map/ppermute | solution.py:48
  35.9 3.1 %fusion.3 = f32[1024]{0:T(1024)S(1)} fusion(bf16[1024,2048]{1,0:T(8,128)(2,1)} %param.14), kind=kLoop, calls=%fused_computation.8 | loop fusion | flops 6290432 | bytes 4198400 | tf_op jit(solution)/shard_map/reduce_sum | solution.py:16
  39.0 4.2 %convolution_convert_fusion.2 = bf16[1024,512]{0,1:T(8,128)(2,1)S(1)} fusion(bf16[2048,512]{1,0:T(8,128)(2,1)} %param.19, bf16[1024,2048]{1,0:T(8,128)(2,1)S(1)} %copy-done.2, f32[2048]{0:T(1024)S(1)} %copy-done.14, f32[1024]{0:T(1024)S(1)} %add_rsqrt_fusion.1), kind=kOutput, calls=%fused_computation.63 | convolution fusion | flops 2156396544 | bytes 7352320 | tf_op jit(solution)/shard_map/dot_general | solution.py:24
  43.2 0.0 copy-start.13
  43.2 1.6 %copy.83 = f32[1024,2,256]{2,0,1:T(8,128)} copy(bf16[1024,2,256]{0,2,1:T(8,128)(2,1)S(1)} %bitcast.23) | data formatting | bytes 3145728 | tf_op jit(solution)/shard_map/reshape | solution.py:25
  44.8 18.1 %convolution_convert_fusion.1 = bf16[2,1024,256]{1,2,0:T(8,128)(2,1)} fusion(bf16[2,256,256]{2,1,0:T(8,128)(2,1)S(1)} %copy-done.13, f32[1024,2,256]{2,0,1:T(8,128)} %copy.83, f32[1024,2]{0,1:T(2,128)S(1)} %minimum_convert_fusion, f32[2]{0:T(128)S(1)} %get-tuple-element.17, f32[2]{0:T(128)S(1)} %get-tuple-element.18, f32[2]{0:T(128)S(1)} %get-tuple-element.19, ...), kind=kOutput, calls=%fused_computation.62 | convolution fusion | flops 286785536 | bytes 3416192 | tf_op jit(solution)/shard_map/tgc,gcd->tgd/dot_general | solution.py:35
  62.9 0.4 collective-permute-start
  63.3 0.1 constant_dynamic-slice_fusion.1
  63.4 0.0 copy-start.3
  63.5 0.2 collective-permute-start.1
  63.7 4.0 %fusion.39 = bf16[1024,1024]{1,0:T(8,128)(2,1)} fusion(bf16[1024,512]{0,1:T(8,128)(2,1)} %bitcast.7, bf16[512,2048]{1,0:T(8,128)(2,1)S(1)} %copy-done, s32[]{:T(128)S(6)} %select_n.528), kind=kOutput, calls=%fused_computation.65 | convolution fusion | flops 1073741824 | bytes 4194308 | tf_op jit(solution)/shard_map/dot_general | solution.py:41
  67.7 2.1 %convolution_convert_fusion.3.q_ref = bf16[1024,256]{1,0:T(8,128)(2,1)} fusion(bf16[2048,256]{1,0:T(8,128)(2,1)S(1)} %copy-done.12, bf16[1024,2048]{1,0:T(8,128)(2,1)S(1)} %copy-done.3, f32[2048]{0:T(1024)S(1)} %copy-done.14, f32[1024]{0:T(1024)S(1)} %add_rsqrt_fusion.1), kind=kOutput, calls=%fused_computation.64 | convolution fusion | flops 1082392576 | bytes 5779456 | tf_op jit(solution)/shard_map/dot_general | solution.py:150
  69.8 0.1 copy-done.9
  69.9 6.3 %fusion.50 = f32[1024,1024]{1,0:T(8,128)} fusion(bf16[2048,1024]{1,0:T(8,128)(2,1)S(1)} %copy-done.9, bf16[1024,2048]{1,0:T(8,128)(2,1)S(1)} %copy-done.3, f32[2048]{0:T(1024)S(1)} %copy-done.14, f32[1024]{0:T(1024)S(1)} %add_rsqrt_fusion.1), kind=kOutput, calls=%fused_computation.116 | convolution fusion | flops 4303355904 | bytes 12595200 | tf_op jit(solution)/shard_map/dot_general | solution.py:149
  76.2 49.9 %all-to-all-done.1.refs_0_.refs_1_.refs_2_.refs_3_ = bf16[64,64,512]{2,1,0:T(8,128)(2,1)} async-done(((bf16[64,64,512]{2,1,0:T(8,128)(2,1)}), bf16[64,64,512]{2,1,0:T(8,128)(2,1)}, u32[]{:S(2)}, u32[]{:S(2)}) %all-to-all-start.1) | async-done | bytes 4194336 | tf_op jit(solution)/shard_map/all_to_all | solution.py:141
  126.1 9.4 %shard_map.136 = bf16[1024,256]{1,0:T(8,128)(2,1)} custom-call(s32[32]{0:T(128)} %copy-done.8, f32[2]{0:T(128)} %broadcast_multiply_fusion.scale_ref, bf16[1024,256]{1,0:T(8,128)(2,1)} %convolution_convert_fusion.3.q_ref, bf16[64,64,512]{2,1,0:T(8,128)(2,1)} %all-to-all-done.1.refs_0_.refs_1_.refs_2_.refs_3_, ...), custom_call_target="tpu_custom_call" | custom-call | flops 268435456 | bytes 4194304 | tf_op jit(solution)/shard_map/pallas_call | solution.py:85
  135.5 1.5 %collective-permute-start.2 = (bf16[1024,256]{1,0:T(8,128)(2,1)}, bf16[1024,256]{1,0:T(8,128)(2,1)S(1)}, u32[]{:S(2)}, u32[]{:S(2)}) collective-permute-start(bf16[1024,256]{1,0:T(8,128)(2,1)} %shard_map.136), channel_id=1, source_target_pairs={{0,1},{1,0},{2,3},{3,2},{4,5},{5,4},{6,7},{7,6},{8,9},{9,8},{10,11... | collective-permute-start | bytes 1572872 | tf_op jit(solution)/shard_map/ppermute | solution.py:48
  137.0 3.0 %fusion.53 = bf16[1024,1024]{1,0:T(8,128)(2,1)S(1)} fusion(bf16[1024,512]{0,1:T(8,128)(2,1)} %collective-permute-done, bf16[512,1024]{1,0:T(8,128)(2,1)} %collective-permute-done.1), kind=kOutput, calls=%fused_computation.117 | convolution fusion | flops 1073741824 | bytes 4194304 | tf_op jit(solution)/shard_map/dot_general | solution.py:41
  140.0 0.0 copy-start.16
  140.0 0.7 fusion.41
  140.8 0.8 copy-done.16
  141.6 4.1 %add_convert_fusion = bf16[1024,1024]{1,0:T(8,128)(2,1)} fusion(f32[1024,1024]{1,0:T(8,128)S(1)} %copy-done.17, bf16[1024,1024]{1,0:T(8,128)(2,1)S(1)} %fusion.41, bf16[1024,1024]{1,0:T(8,128)(2,1)S(1)} %fusion.53, bf16[1024,1024]{1,0:T(8,128)(2,1)S(1)} %copy-done.16, bf16[1024,256]{1,0:T(8,128)(2,1)S(1)} %collective-permute-done.2, ...), kind=kOutput, calls=%fused_computation.11 | convolution fusion | flops 550502400 | bytes 13631488 | tf_op jit(solution)/shard_map/dot_general | solution.py:41
  (49 shorter events, 0.2 us)
Async XLA Ops:
  0.0 63.3 %copy-start = (bf16[512,2048]{1,0:T(8,128)(2,1)S(1)}, bf16[512,2048]{1,0:T(8,128)(2,1)}, u32[]{:S(2)}) copy-start(bf16[512,2048]{1,0:T(8,128)(2,1)} %param.21) | copy-start | bytes 6291460
  2.3 11.6 %copy-start.8 = (s32[32]{0:T(128)}, s32[32]{0:T(128)S(1)}, u32[]{:S(2)}) copy-start(s32[32]{0:T(128)S(1)} %multiply_add_fusion.slots_ref) | copy-start | bytes 388
  3.0 17.5 %all-to-all-start = ((s32[16,1,4]{2,1,0:T(1,128)}), s32[16,1,4]{2,1,0:T(1,128)S(1)}, u32[]{:S(2)}, u32[]{:S(2)}) async-start(s32[16,1,4]{2,1,0:T(1,128)} %bitcast.2), calls=%async_computation | async-start | bytes 16384 | tf_op jit(solution)/shard_map/all_to_all | solution.py:133
  9.6 4.6 %copy-start.1 = (bf16[24,64,2048]{2,1,0:T(8,128)(2,1)S(1)}, bf16[24,64,2048]{2,1,0:T(8,128)(2,1)}, u32[]{:S(2)}) copy-start(bf16[24,64,2048]{2,1,0:T(8,128)(2,1)} %param.16) | copy-start | bytes 18874372
  9.6 4.6 %copy-start.7 = (f32[2048]{0:T(1024)S(1)}, f32[2048]{0:T(1024)}, u32[]{:S(2)}) copy-start(f32[2048]{0:T(1024)} %param.17) | copy-start | bytes 24580
  14.2 1.5 %copy-start.10 = (bf16[2048,256]{1,0:T(8,128)(2,1)S(1)}, bf16[2048,256]{1,0:T(8,128)(2,1)}, u32[]{:S(2)}) copy-start(bf16[2048,256]{1,0:T(8,128)(2,1)} %param.24) | copy-start | bytes 3145732
  14.2 1.5 %copy-start.11 = (bf16[2048,256]{1,0:T(8,128)(2,1)S(1)}, bf16[2048,256]{1,0:T(8,128)(2,1)}, u32[]{:S(2)}) copy-start(bf16[2048,256]{1,0:T(8,128)(2,1)} %param.23) | copy-start | bytes 3145732
  26.0 6.7 %copy-start.15 = (f32[2]{0:T(128)S(1)}, f32[2]{0:T(128)}, u32[]{:S(2)}) copy-start(f32[2]{0:T(128)} %param.25) | copy-start | bytes 28
  26.0 7.2 %copy-start.5 = (bf16[256,2048]{1,0:T(8,128)(2,1)S(1)}, bf16[256,2048]{1,0:T(8,128)(2,1)}, u32[]{:S(2)}) copy-start(bf16[256,2048]{1,0:T(8,128)(2,1)} %param.26) | copy-start | bytes 3145732
  26.0 100.1 %all-to-all-start.1 = ((bf16[64,64,512]{2,1,0:T(8,128)(2,1)}), bf16[64,64,512]{2,1,0:T(8,128)(2,1)}, u32[]{:S(2)}, u32[]{:S(2)}) async-start(bf16[64,64,512]{2,1,0:T(8,128)(2,1)} %gather_fusion), calls=%async_computation.1 | async-start | bytes 8388608 | tf_op jit(solution)/shard_map/all_to_all | solution.py:141
  34.1 4.9 %copy-start.2 = (bf16[1024,2048]{1,0:T(8,128)(2,1)S(1)}, bf16[1024,2048]{1,0:T(8,128)(2,1)}, u32[]{:S(2)}) copy-start(bf16[1024,2048]{1,0:T(8,128)(2,1)} %param.14) | copy-start | bytes 12582916
  34.1 4.9 %copy-start.14 = (f32[2048]{0:T(1024)S(1)}, f32[2048]{0:T(1024)}, u32[]{:S(2)}) copy-start(f32[2048]{0:T(1024)} %param.15) | copy-start | bytes 24580
  34.1 106.6 %collective-permute-start.3 = (bf16[256,1024]{1,0:T(8,128)(2,1)}, bf16[256,1024]{1,0:T(8,128)(2,1)}, u32[]{:S(2)}, u32[]{:S(2)}) collective-permute-start(bf16[256,1024]{1,0:T(8,128)(2,1)} %constant_dynamic-slice_fusion), channel_id=1, source_target_pairs={{0,1},{1,0},{2,3},{3,2},{4,5},{5,4},{6,7},{7,6},{8,9},{9,8},{10,11... | collective-permute-start | bytes 1572872 | tf_op jit(solution)/shard_map/ppermute | solution.py:48
  43.2 1.6 %copy-start.13 = (bf16[2,256,256]{2,1,0:T(8,128)(2,1)S(1)}, bf16[2,256,256]{2,1,0:T(8,128)(2,1)}, u32[]{:S(2)}) copy-start(bf16[2,256,256]{2,1,0:T(8,128)(2,1)} %param.20) | copy-start | bytes 786436
  62.9 74.0 %collective-permute-start = (bf16[1024,512]{0,1:T(8,128)(2,1)}, bf16[1024,512]{0,1:T(8,128)(2,1)}, u32[]{:S(2)}, u32[]{:S(2)}) collective-permute-start(bf16[1024,512]{0,1:T(8,128)(2,1)} %bitcast.7), channel_id=1, source_target_pairs={{0,1},{1,0},{2,3},{3,2},{4,5},{5,4},{6,7},{7,6},{8,9},{9,8},{10,11... | collective-permute-start | bytes 3145736 | tf_op jit(solution)/shard_map/ppermute | solution.py:48
  63.4 4.2 %copy-start.3 = (bf16[1024,2048]{1,0:T(8,128)(2,1)S(1)}, bf16[1024,2048]{1,0:T(8,128)(2,1)}, u32[]{:S(2)}) copy-start(bf16[1024,2048]{1,0:T(8,128)(2,1)} %param.14) | copy-start | bytes 12582916
  63.4 4.2 %copy-start.12 = (bf16[2048,256]{1,0:T(8,128)(2,1)S(1)}, bf16[2048,256]{1,0:T(8,128)(2,1)}, u32[]{:S(2)}) copy-start(bf16[2048,256]{1,0:T(8,128)(2,1)} %param.22) | copy-start | bytes 3145732
  63.5 73.5 %collective-permute-start.1 = (bf16[512,1024]{1,0:T(8,128)(2,1)S(1)}, bf16[512,1024]{1,0:T(8,128)(2,1)}, u32[]{:S(2)}, u32[]{:S(2)}) collective-permute-start(bf16[512,1024]{1,0:T(8,128)(2,1)S(1)} %constant_dynamic-slice_fusion.1), channel_id=1, source_target_pairs={{0,1},{1,0},{2,3},{3,2},{4,5},{5,4},{6,7},{7,6},{8,9},{9,8},{10,11... | collective-permute-start | bytes 3145736 | tf_op jit(solution)/shard_map/ppermute | solution.py:48
  67.7 2.2 %copy-start.9 = (bf16[2048,1024]{1,0:T(8,128)(2,1)S(1)}, bf16[2048,1024]{1,0:T(8,128)(2,1)}, u32[]{:S(2)}) copy-start(bf16[2048,1024]{1,0:T(8,128)(2,1)} %param.27) | copy-start | bytes 12582916
  135.5 4.5 %copy-start.4 = (bf16[1024,256]{1,0:T(8,128)(2,1)S(1)}, bf16[1024,256]{1,0:T(8,128)(2,1)}, u32[]{:S(2)}) copy-start(bf16[1024,256]{1,0:T(8,128)(2,1)} %shard_map.136) | copy-start | bytes 1572868
  135.5 4.5 %copy-start.6 = (bf16[256,2048]{1,0:T(8,128)(2,1)S(1)}, bf16[256,2048]{1,0:T(8,128)(2,1)}, u32[]{:S(2)}) copy-start(bf16[256,2048]{1,0:T(8,128)(2,1)} %param.26) | copy-start | bytes 3145732
  135.5 5.2 %collective-permute-start.2 = (bf16[1024,256]{1,0:T(8,128)(2,1)}, bf16[1024,256]{1,0:T(8,128)(2,1)S(1)}, u32[]{:S(2)}, u32[]{:S(2)}) collective-permute-start(bf16[1024,256]{1,0:T(8,128)(2,1)} %shard_map.136), channel_id=1, source_target_pairs={{0,1},{1,0},{2,3},{3,2},{4,5},{5,4},{6,7},{7,6},{8,9},{9,8},{10,11... | collective-permute-start | bytes 1572872 | tf_op jit(solution)/shard_map/ppermute | solution.py:48
  137.0 3.8 %copy-start.17 = (f32[1024,1024]{1,0:T(8,128)S(1)}, f32[1024,1024]{1,0:T(8,128)}, u32[]{:S(2)}) copy-start(f32[1024,1024]{1,0:T(8,128)} %fusion.50) | copy-start | bytes 12582916
  140.0 1.6 %copy-start.16 = (bf16[1024,1024]{1,0:T(8,128)(2,1)S(1)}, bf16[1024,1024]{1,0:T(8,128)(2,1)}, u32[]{:S(2)}) copy-start(bf16[1024,1024]{1,0:T(8,128)(2,1)} %fusion.39) | copy-start | bytes 6291460
where the time goes:
time: 147 us; the launch traced here: 146 us
  waiting for transfers between devices  49.9 us (34%)
  matrix products  47.2 us (32%)
  starting transfers between devices  17 us (12%)
  other arithmetic  12 us (8%)
  local copies, waits for them, and re-layouts  9.85 us (7%)
  Pallas kernels  9.4 us (6%)
    all_to_all x1, waiting for transfers between devices, body(): kv = lax.all_to_all(packed, 'st', split_axis=0, concat_axis=0, tiled=True)  49.9 us
    dot_general x1, matrix products, pool_branch(): jnp.einsum('tgc,gcd->tgd', pooled, pool_mix, preferred_element_type=jnp.f...  18.1 us
    dot_general x4, matrix products, half_terms(): jnp.dot(a, w, preferred_element_type=jnp.float32).astype(jnp.bfloat16)  11.8 us
    pallas_call x1, Pallas kernels, attend(): pl.pallas_call(functools.partial(attention_kernel, heads), out_shape=jax....  9.4 us
    reduce_sum x2, other arithmetic, rms_norm(): scale = lax.rsqrt(jnp.mean(wide * wide, axis=-1, keepdims=True) + 1e-05)  7.3 us
    all_to_all x1, starting transfers between devices, body(): lax.all_to_all(request, 'st', split_axis=0, concat_axis=0, tiled=True)  6.58 us
    all_to_all x1, starting transfers between devices, body(): kv = lax.all_to_all(packed, 'st', split_axis=0, concat_axis=0, tiled=True)  6.49 us
    dot_general x1, matrix products, body(): jnp.dot(normed, w_gate, preferred_element_type=jnp.float32)  6.29 us
  transfers between devices with their start and end apart: 6, of which 1 were waited for; matrix products, arithmetic and copies ran while one was open for 38% of the time, Pallas kernels for 6%

commit v1 on v0

--- a/solution.py
+++ b/solution.py
@@ -9,6 +9,8 @@
 from jax.sharding import PartitionSpec as P
 
 GROUPS = 4
+ATTEND_BLOCKS = 2
+MESH = pl.DeviceIdType.MESH
 
 
 def rms_norm(values, gain):
@@ -53,20 +55,23 @@
     return lax.dynamic_slice_in_dim(weight, part * half, half, axis=1)
 
 
-def attention_kernel(heads, slots_ref, scale_ref, q_ref, *refs):
+def attention_kernel(heads, group, slots_ref, scale_ref, q_ref, *refs):
     parts, out_ref = refs[:-1], refs[-1]
-    kv = jnp.concatenate([r[0] for r in parts], axis=0)
     width = q_ref.shape[1]
     head_dim = width // heads
-    for h in range(heads):
+    block_len = q_ref.shape[0] // group
+    per_block = len(parts) // group
+    for b, h in [(b, h) for b in range(group) for h in range(heads)]:
+        rows = slice(b * block_len, (b + 1) * block_len)
+        kv = jnp.concatenate([r[0] for r in parts[b * per_block : (b + 1) * per_block]], axis=0)
         cut = slice(h * head_dim, (h + 1) * head_dim)
         scores = lax.dot_general(
-            q_ref[:, cut], kv[:, cut], (((1,), (1,)), ((), ())), preferred_element_type=jnp.float32
+            q_ref[rows, cut], kv[:, cut], (((1,), (1,)), ((), ())), preferred_element_type=jnp.float32
         )
         scores = scores * scale_ref[h]
         top = jnp.exp(scores - jnp.max(scores, axis=-1, keepdims=True))
-        weights = (top / jnp.sum(top, axis=-1, keepdims=True)).astype(jnp.bfloat16)
-        out_ref[:, cut] = jnp.dot(
+        weights = (top * (1.0 / jnp.sum(top, axis=-1, keepdims=True))).astype(jnp.bfloat16)
+        out_ref[rows, cut] = jnp.dot(
             weights, kv[:, width + h * head_dim : width + (h + 1) * head_dim],
             preferred_element_type=jnp.float32,
         ).astype(jnp.bfloat16)
@@ -78,26 +83,28 @@
     block_len = tokens // blocks_dev
     length, both = kv.shape[1:]
     heads = scale.shape[0]
+    group = math.gcd(blocks_dev, ATTEND_BLOCKS)
+    taken = group * per_block
 
     def part(j):
-        return pl.BlockSpec((1, length, both), lambda b, slots: (slots[b * per_block + j], 0, 0))
+        return pl.BlockSpec((1, length, both), lambda b, slots: (slots[b * taken + j], 0, 0))
 
     return pl.pallas_call(
-        functools.partial(attention_kernel, heads),
+        functools.partial(attention_kernel, heads, group),
         out_shape=jax.ShapeDtypeStruct((tokens, width), jnp.bfloat16),
         grid_spec=pltpu.PrefetchScalarGridSpec(
             num_scalar_prefetch=1,
-            grid=(blocks_dev,),
+            grid=(blocks_dev // group,),
             in_specs=[
                 pl.BlockSpec(memory_space=pltpu.SMEM),
-                pl.BlockSpec((block_len, width), lambda b, slots: (b, 0)),
-            ] + [part(j) for j in range(per_block)],
-            out_specs=pl.BlockSpec((block_len, width), lambda b, slots: (b, 0)),
+                pl.BlockSpec((group * block_len, width), lambda b, slots: (b, 0)),
+            ] + [part(j) for j in range(taken)],
+            out_specs=pl.BlockSpec((group * block_len, width), lambda b, slots: (b, 0)),
         ),
         cost_estimate=pl.CostEstimate(
             flops=4 * tokens * per_block * length * width, bytes_accessed=4 * 2**20, transcendentals=0
         ),
-    )(block_slot.reshape(-1), scale, query, *([kv] * per_block))
+    )(block_slot.reshape(-1), scale, query, *([kv] * taken))
 
 
 def body(
@@ -121,8 +128,8 @@
     flat_ids = passage_ids.reshape(-1)
     reads = flat_ids.shape[0]
     pass_dev, length, width = store.shape
-    owner = flat_ids // pass_dev
-    local = flat_ids % pass_dev
+    owner = lax.div(flat_ids, pass_dev)
+    local = flat_ids - owner * pass_dev
     order = jnp.arange(reads, dtype=jnp.int32)
     earlier = (owner[None, :] == owner[:, None]) & (order[None, :] < order[:, None])
     rank = jnp.sum(earlier.astype(jnp.int32), axis=1)

time: 147 us -> 142 us (0.966)
  Pallas kernels: 9.4 us -> 6.53 us
  other arithmetic: 12 us -> 10.5 us
    pallas_call x1, Pallas kernels: 9.4 us -> 6.53 us  [attend(): pl.pallas_call(functools.partial(attention_kernel, heads, group), out_sha...]
  transfers between devices with their start and end apart: 6 -> 6, of which waited for: 1 -> 1; matrix products, arithmetic and copies ran while one was open for 38% -> 39% of each run, Pallas kernels for 6% -> 5%
where the time goes in v1:
time: 142 us
  waiting for transfers between devices  49.9 us (35%)
  matrix products  47.2 us (33%)
  starting transfers between devices  17 us (12%)
  other arithmetic  10.5 us (7%)
  local copies, waits for them, and re-layouts  10.4 us (7%)
  Pallas kernels  6.53 us (5%)
    all_to_all x1, waiting for transfers between devices, body(): kv = lax.all_to_all(packed, 'st', split_axis=0, concat_axis=0, tiled=True)  49.8 us
    dot_general x1, matrix products, pool_branch(): jnp.einsum('tgc,gcd->tgd', pooled, pool_mix, preferred_element_type=jnp.f...  18.1 us
    dot_general x4, matrix products, half_terms(): jnp.dot(a, w, preferred_element_type=jnp.float32).astype(jnp.bfloat16)  11.8 us
    reduce_sum x2, other arithmetic, rms_norm(): scale = lax.rsqrt(jnp.mean(wide * wide, axis=-1, keepdims=True) + 1e-05)  7.3 us
    all_to_all x1, starting transfers between devices, body(): lax.all_to_all(request, 'st', split_axis=0, concat_axis=0, tiled=True)  6.58 us
    pallas_call x1, Pallas kernels, attend(): pl.pallas_call(functools.partial(attention_kernel, heads, group), out_sha...  6.53 us
    all_to_all x1, starting transfers between devices, body(): kv = lax.all_to_all(packed, 'st', split_axis=0, concat_axis=0, tiled=True)  6.49 us
    dot_general x1, matrix products, body(): jnp.dot(normed, w_gate, preferred_element_type=jnp.float32)  6.27 us
  transfers between devices with their start and end apart: 6, of which 1 were waited for; matrix products, arithmetic and copies ran while one was open for 39% of the time, Pallas kernels for 5%

profile of v1, /device:TPU:15, one launch (start us, length us, event | category | flops | bytes accessed | tf_op | source)
XLA Modules:
  0.0 141.6 jit_solution(15002603463192582285)
XLA Ops:
  0.0 0.9 copy.73
  0.9 0.1 reshape.258
  1.0 0.2 convert_reduce_fusion
  1.2 0.1 select_reduce_fusion
  1.3 0.7 all_to_all.9
  2.0 6.6 %all-to-all-start = ((s32[16,1,4]{2,1,0:T(1,128)}), s32[16,1,4]{2,1,0:T(1,128)S(1)}, u32[]{:S(2)}, u32[]{:S(2)}) async-start(s32[16,1,4]{2,1,0:T(1,128)} %bitcast.2), calls=%async_computation | async-start | bytes 16384 | tf_op jit(solution)/shard_map/all_to_all | solution.py:140
  8.6 0.0 copy-start.7
  8.6 4.2 %fusion = f32[24,64]{1,0:T(8,128)S(1)} fusion(bf16[24,64,2048]{2,1,0:T(8,128)(2,1)} %param.16), kind=kLoop, calls=%fused_computation.3 | loop fusion | flops 9435648 | bytes 6297600 | tf_op jit(solution)/shard_map/reduce_sum | solution.py:18
  12.8 0.3 copy-done.1
  13.2 1.5 %fusion.2 = bf16[24,64,2048]{2,1,0:T(8,128)(2,1)S(1)} fusion(bf16[24,64,2048]{2,1,0:T(8,128)(2,1)S(1)} %copy-done.1, f32[2048]{0:T(1024)S(1)} %copy-done.7, f32[24,64]{1,0:T(8,128)S(1)} %add_rsqrt_fusion), kind=kLoop, calls=%fused_computation.5 | loop fusion | flops 12582912 | bytes 12597248 | tf_op jit(solution)/shard_map/convert_element_type | solution.py:142
  14.7 0.0 copy-done.11
  14.7 4.8 %convolution_convert_fusion = bf16[1536,512]{1,0:T(8,128)(2,1)} fusion(bf16[1536,2048]{1,0:T(8,128)(2,1)S(1)} %bitcast.22, bf16[2048,256]{1,0:T(8,128)(2,1)S(1)} %copy-done.10, bf16[2048,256]{1,0:T(8,128)(2,1)S(1)} %copy-done.11), kind=kOutput, calls=%fused_computation.12 | convolution fusion | flops 3226206208 | bytes 9961472 | tf_op jit(solution)/shard_map/dot_general | solution.py:144
  19.5 0.0 all-to-all-done
  19.5 0.5 broadcast.2008
  20.0 0.6 reduce.3
  20.6 0.1 reshape.259
  20.7 4.2 %gather_fusion = bf16[64,64,512]{2,1,0:T(8,128)(2,1)} fusion(bf16[24,64,512]{2,1,0:T(8,128)(2,1)} %bitcast.21, s32[1024]{0:T(1024)S(1)} %pad_clamp_fusion), kind=kCustom, calls=%fused_computation | custom fusion | bytes 8388864 | tf_op jit(solution)/shard_map/gather | solution.py:146
  24.9 6.5 %all-to-all-start.1 = ((bf16[64,64,512]{2,1,0:T(8,128)(2,1)}), bf16[64,64,512]{2,1,0:T(8,128)(2,1)}, u32[]{:S(2)}, u32[]{:S(2)}) async-start(bf16[64,64,512]{2,1,0:T(8,128)(2,1)} %gather_fusion), calls=%async_computation.1 | async-start | bytes 8388608 | tf_op jit(solution)/shard_map/all_to_all | solution.py:148
  31.6 0.6 broadcast_multiply_fusion.scale_ref
  32.2 0.1 minimum_convert_fusion
  32.2 0.9 constant_dynamic-slice_fusion
  33.1 1.8 %collective-permute-start.3 = (bf16[256,1024]{1,0:T(8,128)(2,1)}, bf16[256,1024]{1,0:T(8,128)(2,1)}, u32[]{:S(2)}, u32[]{:S(2)}) collective-permute-start(bf16[256,1024]{1,0:T(8,128)(2,1)} %constant_dynamic-slice_fusion), channel_id=1, source_target_pairs={{0,1},{1,0},{2,3},{3,2},{4,5},{5,4},{6,7},{7,6},{8,9},{9,8},{10,11... | collective-permute-start | bytes 1572872 | tf_op jit(solution)/shard_map/ppermute | solution.py:50
  34.9 3.1 %fusion.3 = f32[1024]{0:T(1024)S(1)} fusion(bf16[1024,2048]{1,0:T(8,128)(2,1)} %param.14), kind=kLoop, calls=%fused_computation.8 | loop fusion | flops 6290432 | bytes 4198400 | tf_op jit(solution)/shard_map/reduce_sum | solution.py:18
  38.0 4.2 %convolution_convert_fusion.2 = bf16[1024,512]{0,1:T(8,128)(2,1)S(1)} fusion(bf16[2048,512]{1,0:T(8,128)(2,1)} %param.19, bf16[1024,2048]{1,0:T(8,128)(2,1)S(1)} %copy-done.2, f32[2048]{0:T(1024)S(1)} %copy-done.14, f32[1024]{0:T(1024)S(1)} %add_rsqrt_fusion.1), kind=kOutput, calls=%fused_computation.63 | convolution fusion | flops 2156396544 | bytes 7352320 | tf_op jit(solution)/shard_map/dot_general | solution.py:26
  42.2 0.0 copy-start.13
  42.2 1.6 %copy.75 = f32[1024,2,256]{2,0,1:T(8,128)} copy(bf16[1024,2,256]{0,2,1:T(8,128)(2,1)S(1)} %bitcast.23) | data formatting | bytes 3145728 | tf_op jit(solution)/shard_map/reshape | solution.py:27
  43.8 18.1 %convolution_convert_fusion.1 = bf16[2,1024,256]{1,2,0:T(8,128)(2,1)} fusion(bf16[2,256,256]{2,1,0:T(8,128)(2,1)S(1)} %copy-done.13, f32[1024,2,256]{2,0,1:T(8,128)} %copy.75, f32[1024,2]{0,1:T(2,128)S(1)} %minimum_convert_fusion, f32[2]{0:T(128)S(1)} %get-tuple-element.15, f32[2]{0:T(128)S(1)} %get-tuple-element.16, f32[2]{0:T(128)S(1)} %get-tuple-element.17, ...), kind=kOutput, calls=%fused_computation.62 | convolution fusion | flops 286785536 | bytes 3416192 | tf_op jit(solution)/shard_map/tgc,gcd->tgd/dot_general | solution.py:37
  61.9 0.4 collective-permute-start
  62.3 0.1 constant_dynamic-slice_fusion.1
  62.4 0.0 copy-start.3
  62.4 0.0 copy-start.12
  62.4 0.2 collective-permute-start.1
  62.7 4.0 %fusion.39 = bf16[1024,1024]{1,0:T(8,128)(2,1)} fusion(bf16[1024,512]{0,1:T(8,128)(2,1)} %bitcast.7, bf16[512,2048]{1,0:T(8,128)(2,1)S(1)} %copy-done, s32[]{:T(128)S(6)} %select_n.499), kind=kOutput, calls=%fused_computation.65 | convolution fusion | flops 1073741824 | bytes 4194308 | tf_op jit(solution)/shard_map/dot_general | solution.py:43
  66.7 2.1 %convolution_convert_fusion.3.q_ref = bf16[1024,256]{1,0:T(8,128)(2,1)} fusion(bf16[2048,256]{1,0:T(8,128)(2,1)S(1)} %copy-done.12, bf16[1024,2048]{1,0:T(8,128)(2,1)S(1)} %copy-done.3, f32[2048]{0:T(1024)S(1)} %copy-done.14, f32[1024]{0:T(1024)S(1)} %add_rsqrt_fusion.1), kind=kOutput, calls=%fused_computation.64 | convolution fusion | flops 1082392576 | bytes 5779456 | tf_op jit(solution)/shard_map/dot_general | solution.py:157
  68.8 0.1 copy-done.9
  68.8 6.3 %fusion.50 = f32[1024,1024]{1,0:T(8,128)} fusion(bf16[2048,1024]{1,0:T(8,128)(2,1)S(1)} %copy-done.9, bf16[1024,2048]{1,0:T(8,128)(2,1)S(1)} %copy-done.3, f32[2048]{0:T(1024)S(1)} %copy-done.14, f32[1024]{0:T(1024)S(1)} %add_rsqrt_fusion.1), kind=kOutput, calls=%fused_computation.113 | convolution fusion | flops 4303355904 | bytes 12595200 | tf_op jit(solution)/shard_map/dot_general | solution.py:156
  75.1 49.8 %all-to-all-done.1.refs_0_.refs_1_.refs_2_.refs_3_.refs_4_.refs_5_.refs_6_.refs_7_ = bf16[64,64,512]{2,1,0:T(8,128)(2,1)} async-done(((bf16[64,64,512]{2,1,0:T(8,128)(2,1)}), bf16[64,64,512]{2,1,0:T(8,128)(2,1)}, u32[]{:S(2)}, u32[]{:S(2)}) %all-to-all-start.1) | async-done | bytes 4194336 | tf_op jit(solution)/shard_map/all_to_all | solution.py:148
  125.0 6.5 %shard_map.136 = bf16[1024,256]{1,0:T(8,128)(2,1)} custom-call(s32[32]{0:T(128)} %copy-done.8, f32[2]{0:T(128)} %broadcast_multiply_fusion.scale_ref, bf16[1024,256]{1,0:T(8,128)(2,1)} %convolution_convert_fusion.3.q_ref, bf16[64,64,512]{2,1,0:T(8,128)(2,1)} %all-to-all-done.1.refs_0_.refs_1_.refs_2_.refs_3_.refs_4_.refs_5_.refs_6_.refs_7_, ...), custom_call_target="tpu_custom_call" | custom-call | flops 268435456 | bytes 4194304 | tf_op jit(solution)/shard_map/pallas_call | solution.py:92
  131.5 0.0 copy-start.6
  131.5 1.5 %collective-permute-start.2 = (bf16[1024,256]{1,0:T(8,128)(2,1)}, bf16[1024,256]{1,0:T(8,128)(2,1)S(1)}, u32[]{:S(2)}, u32[]{:S(2)}) collective-permute-start(bf16[1024,256]{1,0:T(8,128)(2,1)} %shard_map.136), channel_id=1, source_target_pairs={{0,1},{1,0},{2,3},{3,2},{4,5},{5,4},{6,7},{7,6},{8,9},{9,8},{10,11... | collective-permute-start | bytes 1572872 | tf_op jit(solution)/shard_map/ppermute | solution.py:50
  133.0 0.0 collective-permute-done.1
  133.0 3.0 %fusion.53 = bf16[1024,1024]{1,0:T(8,128)(2,1)S(1)} fusion(bf16[1024,512]{0,1:T(8,128)(2,1)} %collective-permute-done, bf16[512,1024]{1,0:T(8,128)(2,1)} %collective-permute-done.1), kind=kOutput, calls=%fused_computation.114 | convolution fusion | flops 1073741824 | bytes 4194304 | tf_op jit(solution)/shard_map/dot_general | solution.py:43
  136.0 0.0 copy-start.16
  136.0 0.7 fusion.41
  136.7 0.0 collective-permute-done.3
  136.7 0.0 collective-permute-done.2
  136.8 0.8 copy-done.16
  137.6 4.1 %add_convert_fusion = bf16[1024,1024]{1,0:T(8,128)(2,1)} fusion(f32[1024,1024]{1,0:T(8,128)S(1)} %copy-done.17, bf16[1024,1024]{1,0:T(8,128)(2,1)S(1)} %fusion.41, bf16[1024,1024]{1,0:T(8,128)(2,1)S(1)} %fusion.53, bf16[1024,1024]{1,0:T(8,128)(2,1)S(1)} %copy-done.16, bf16[1024,256]{1,0:T(8,128)(2,1)S(1)} %collective-permute-done.2, ...), kind=kOutput, calls=%fused_computation.11 | convolution fusion | flops 550502400 | bytes 13631488 | tf_op jit(solution)/shard_map/dot_general | solution.py:43
  (43 shorter events, 0.2 us)
Async XLA Ops:
  0.0 62.3 %copy-start = (bf16[512,2048]{1,0:T(8,128)(2,1)S(1)}, bf16[512,2048]{1,0:T(8,128)(2,1)}, u32[]{:S(2)}) copy-start(bf16[512,2048]{1,0:T(8,128)(2,1)} %param.21) | copy-start | bytes 6291460
  1.2 11.6 %copy-start.8 = (s32[32]{0:T(128)}, s32[32]{0:T(128)S(1)}, u32[]{:S(2)}) copy-start(s32[32]{0:T(128)S(1)} %multiply_add_fusion.slots_ref) | copy-start | bytes 388
  2.0 17.5 %all-to-all-start = ((s32[16,1,4]{2,1,0:T(1,128)}), s32[16,1,4]{2,1,0:T(1,128)S(1)}, u32[]{:S(2)}, u32[]{:S(2)}) async-start(s32[16,1,4]{2,1,0:T(1,128)} %bitcast.2), calls=%async_computation | async-start | bytes 16384 | tf_op jit(solution)/shard_map/all_to_all | solution.py:140
  8.6 4.6 %copy-start.1 = (bf16[24,64,2048]{2,1,0:T(8,128)(2,1)S(1)}, bf16[24,64,2048]{2,1,0:T(8,128)(2,1)}, u32[]{:S(2)}) copy-start(bf16[24,64,2048]{2,1,0:T(8,128)(2,1)} %param.16) | copy-start | bytes 18874372
  8.6 4.6 %copy-start.7 = (f32[2048]{0:T(1024)S(1)}, f32[2048]{0:T(1024)}, u32[]{:S(2)}) copy-start(f32[2048]{0:T(1024)} %param.17) | copy-start | bytes 24580
  13.2 1.5 %copy-start.10 = (bf16[2048,256]{1,0:T(8,128)(2,1)S(1)}, bf16[2048,256]{1,0:T(8,128)(2,1)}, u32[]{:S(2)}) copy-start(bf16[2048,256]{1,0:T(8,128)(2,1)} %param.24) | copy-start | bytes 3145732
  13.2 1.5 %copy-start.11 = (bf16[2048,256]{1,0:T(8,128)(2,1)S(1)}, bf16[2048,256]{1,0:T(8,128)(2,1)}, u32[]{:S(2)}) copy-start(bf16[2048,256]{1,0:T(8,128)(2,1)} %param.23) | copy-start | bytes 3145732
  24.9 6.7 %copy-start.15 = (f32[2]{0:T(128)S(1)}, f32[2]{0:T(128)}, u32[]{:S(2)}) copy-start(f32[2]{0:T(128)} %param.25) | copy-start | bytes 28
  24.9 7.3 %copy-start.5 = (bf16[256,2048]{1,0:T(8,128)(2,1)S(1)}, bf16[256,2048]{1,0:T(8,128)(2,1)}, u32[]{:S(2)}) copy-start(bf16[256,2048]{1,0:T(8,128)(2,1)} %param.26) | copy-start | bytes 3145732
  24.9 100.0 %all-to-all-start.1 = ((bf16[64,64,512]{2,1,0:T(8,128)(2,1)}), bf16[64,64,512]{2,1,0:T(8,128)(2,1)}, u32[]{:S(2)}, u32[]{:S(2)}) async-start(bf16[64,64,512]{2,1,0:T(8,128)(2,1)} %gather_fusion), calls=%async_computation.1 | async-start | bytes 8388608 | tf_op jit(solution)/shard_map/all_to_all | solution.py:148
  33.1 4.9 %copy-start.2 = (bf16[1024,2048]{1,0:T(8,128)(2,1)S(1)}, bf16[1024,2048]{1,0:T(8,128)(2,1)}, u32[]{:S(2)}) copy-start(bf16[1024,2048]{1,0:T(8,128)(2,1)} %param.14) | copy-start | bytes 12582916
  33.1 4.9 %copy-start.14 = (f32[2048]{0:T(1024)S(1)}, f32[2048]{0:T(1024)}, u32[]{:S(2)}) copy-start(f32[2048]{0:T(1024)} %param.15) | copy-start | bytes 24580
  33.1 103.6 %collective-permute-start.3 = (bf16[256,1024]{1,0:T(8,128)(2,1)}, bf16[256,1024]{1,0:T(8,128)(2,1)}, u32[]{:S(2)}, u32[]{:S(2)}) collective-permute-start(bf16[256,1024]{1,0:T(8,128)(2,1)} %constant_dynamic-slice_fusion), channel_id=1, source_target_pairs={{0,1},{1,0},{2,3},{3,2},{4,5},{5,4},{6,7},{7,6},{8,9},{9,8},{10,11... | collective-permute-start | bytes 1572872 | tf_op jit(solution)/shard_map/ppermute | solution.py:50
  42.2 1.6 %copy-start.13 = (bf16[2,256,256]{2,1,0:T(8,128)(2,1)S(1)}, bf16[2,256,256]{2,1,0:T(8,128)(2,1)}, u32[]{:S(2)}) copy-start(bf16[2,256,256]{2,1,0:T(8,128)(2,1)} %param.20) | copy-start | bytes 786436
  61.9 71.1 %collective-permute-start = (bf16[1024,512]{0,1:T(8,128)(2,1)}, bf16[1024,512]{0,1:T(8,128)(2,1)}, u32[]{:S(2)}, u32[]{:S(2)}) collective-permute-start(bf16[1024,512]{0,1:T(8,128)(2,1)} %bitcast.7), channel_id=1, source_target_pairs={{0,1},{1,0},{2,3},{3,2},{4,5},{5,4},{6,7},{7,6},{8,9},{9,8},{10,11... | collective-permute-start | bytes 3145736 | tf_op jit(solution)/shard_map/ppermute | solution.py:50
  62.4 4.3 %copy-start.3 = (bf16[1024,2048]{1,0:T(8,128)(2,1)S(1)}, bf16[1024,2048]{1,0:T(8,128)(2,1)}, u32[]{:S(2)}) copy-start(bf16[1024,2048]{1,0:T(8,128)(2,1)} %param.14) | copy-start | bytes 12582916
  62.4 4.2 %copy-start.12 = (bf16[2048,256]{1,0:T(8,128)(2,1)S(1)}, bf16[2048,256]{1,0:T(8,128)(2,1)}, u32[]{:S(2)}) copy-start(bf16[2048,256]{1,0:T(8,128)(2,1)} %param.22) | copy-start | bytes 3145732
  62.4 70.6 %collective-permute-start.1 = (bf16[512,1024]{1,0:T(8,128)(2,1)S(1)}, bf16[512,1024]{1,0:T(8,128)(2,1)}, u32[]{:S(2)}, u32[]{:S(2)}) collective-permute-start(bf16[512,1024]{1,0:T(8,128)(2,1)S(1)} %constant_dynamic-slice_fusion.1), channel_id=1, source_target_pairs={{0,1},{1,0},{2,3},{3,2},{4,5},{5,4},{6,7},{7,6},{8,9},{9,8},{10,11... | collective-permute-start | bytes 3145736 | tf_op jit(solution)/shard_map/ppermute | solution.py:50
  66.6 2.2 %copy-start.9 = (bf16[2048,1024]{1,0:T(8,128)(2,1)S(1)}, bf16[2048,1024]{1,0:T(8,128)(2,1)}, u32[]{:S(2)}) copy-start(bf16[2048,1024]{1,0:T(8,128)(2,1)} %param.27) | copy-start | bytes 12582916
  131.5 4.5 %copy-start.4 = (bf16[1024,256]{1,0:T(8,128)(2,1)S(1)}, bf16[1024,256]{1,0:T(8,128)(2,1)}, u32[]{:S(2)}) copy-start(bf16[1024,256]{1,0:T(8,128)(2,1)} %shard_map.136) | copy-start | bytes 1572868
  131.5 4.5 %copy-start.6 = (bf16[256,2048]{1,0:T(8,128)(2,1)S(1)}, bf16[256,2048]{1,0:T(8,128)(2,1)}, u32[]{:S(2)}) copy-start(bf16[256,2048]{1,0:T(8,128)(2,1)} %param.26) | copy-start | bytes 3145732
  131.5 5.2 %collective-permute-start.2 = (bf16[1024,256]{1,0:T(8,128)(2,1)}, bf16[1024,256]{1,0:T(8,128)(2,1)S(1)}, u32[]{:S(2)}, u32[]{:S(2)}) collective-permute-start(bf16[1024,256]{1,0:T(8,128)(2,1)} %shard_map.136), channel_id=1, source_target_pairs={{0,1},{1,0},{2,3},{3,2},{4,5},{5,4},{6,7},{7,6},{8,9},{9,8},{10,11... | collective-permute-start | bytes 1572872 | tf_op jit(solution)/shard_map/ppermute | solution.py:50
  133.0 3.8 %copy-start.17 = (f32[1024,1024]{1,0:T(8,128)S(1)}, f32[1024,1024]{1,0:T(8,128)}, u32[]{:S(2)}) copy-start(f32[1024,1024]{1,0:T(8,128)} %fusion.50) | copy-start | bytes 12582916
  136.0 1.6 %copy-start.16 = (bf16[1024,1024]{1,0:T(8,128)(2,1)S(1)}, bf16[1024,1024]{1,0:T(8,128)(2,1)}, u32[]{:S(2)}) copy-start(bf16[1024,1024]{1,0:T(8,128)(2,1)} %fusion.39) | copy-start | bytes 6291460

commit v2 on v1

--- a/solution.py
+++ b/solution.py
@@ -9,7 +9,7 @@
 from jax.sharding import PartitionSpec as P
 
 GROUPS = 4
-ATTEND_BLOCKS = 2
+ATTEND_BLOCKS = 4
 MESH = pl.DeviceIdType.MESH
 
 

time: 142 us -> 141 us (level)
  transfers between devices with their start and end apart: 6 -> 6, of which waited for: 1 -> 1; matrix products, arithmetic and copies ran while one was open for 39% -> 39% of each run, Pallas kernels for 5% -> 4%
where the time goes in v2:
time: 141 us
  waiting for transfers between devices  49.9 us (35%)
  matrix products  47.2 us (33%)
  starting transfers between devices  17 us (12%)
  other arithmetic  10.5 us (7%)
  local copies, waits for them, and re-layouts  10.4 us (7%)
  Pallas kernels  5.54 us (4%)
    all_to_all x1, waiting for transfers between devices, body(): kv = lax.all_to_all(packed, 'st', split_axis=0, concat_axis=0, tiled=True)  49.8 us
    dot_general x1, matrix products, pool_branch(): jnp.einsum('tgc,gcd->tgd', pooled, pool_mix, preferred_element_type=jnp.f...  18.1 us
    dot_general x4, matrix products, half_terms(): jnp.dot(a, w, preferred_element_type=jnp.float32).astype(jnp.bfloat16)  11.8 us
    reduce_sum x2, other arithmetic, rms_norm(): scale = lax.rsqrt(jnp.mean(wide * wide, axis=-1, keepdims=True) + 1e-05)  7.3 us
    all_to_all x1, starting transfers between devices, body(): lax.all_to_all(request, 'st', split_axis=0, concat_axis=0, tiled=True)  6.58 us
    all_to_all x1, starting transfers between devices, body(): kv = lax.all_to_all(packed, 'st', split_axis=0, concat_axis=0, tiled=True)  6.49 us
    dot_general x1, matrix products, body(): jnp.dot(normed, w_gate, preferred_element_type=jnp.float32)  6.27 us
    pallas_call x1, Pallas kernels, attend(): pl.pallas_call(functools.partial(attention_kernel, heads, group), out_sha...  5.54 us
  transfers between devices with their start and end apart: 6, of which 1 were waited for; matrix products, arithmetic and copies ran while one was open for 39% of the time, Pallas kernels for 4%

profile of v2, /device:TPU:15, one launch (start us, length us, event | category | flops | bytes accessed | tf_op | source)
XLA Modules:
  0.0 140.7 jit_solution(11810878679422064396)
XLA Ops:
  0.0 0.9 copy.73
  0.9 0.1 reshape.258
  1.0 0.2 convert_reduce_fusion
  1.2 0.1 select_reduce_fusion
  1.3 0.7 all_to_all.9
  2.0 6.6 %all-to-all-start = ((s32[16,1,4]{2,1,0:T(1,128)}), s32[16,1,4]{2,1,0:T(1,128)S(1)}, u32[]{:S(2)}, u32[]{:S(2)}) async-start(s32[16,1,4]{2,1,0:T(1,128)} %bitcast.2), calls=%async_computation | async-start | bytes 16384 | tf_op jit(solution)/shard_map/all_to_all | solution.py:140
  8.6 0.0 copy-start.7
  8.6 4.2 %fusion = f32[24,64]{1,0:T(8,128)S(1)} fusion(bf16[24,64,2048]{2,1,0:T(8,128)(2,1)} %param.16), kind=kLoop, calls=%fused_computation.3 | loop fusion | flops 9435648 | bytes 6297600 | tf_op jit(solution)/shard_map/reduce_sum | solution.py:18
  12.8 0.3 copy-done.1
  13.2 1.5 %fusion.2 = bf16[24,64,2048]{2,1,0:T(8,128)(2,1)S(1)} fusion(bf16[24,64,2048]{2,1,0:T(8,128)(2,1)S(1)} %copy-done.1, f32[2048]{0:T(1024)S(1)} %copy-done.7, f32[24,64]{1,0:T(8,128)S(1)} %add_rsqrt_fusion), kind=kLoop, calls=%fused_computation.5 | loop fusion | flops 12582912 | bytes 12597248 | tf_op jit(solution)/shard_map/convert_element_type | solution.py:142
  14.7 0.0 copy-done.11
  14.7 4.8 %convolution_convert_fusion = bf16[1536,512]{1,0:T(8,128)(2,1)} fusion(bf16[1536,2048]{1,0:T(8,128)(2,1)S(1)} %bitcast.22, bf16[2048,256]{1,0:T(8,128)(2,1)S(1)} %copy-done.10, bf16[2048,256]{1,0:T(8,128)(2,1)S(1)} %copy-done.11), kind=kOutput, calls=%fused_computation.12 | convolution fusion | flops 3226206208 | bytes 9961472 | tf_op jit(solution)/shard_map/dot_general | solution.py:144
  19.5 0.0 all-to-all-done
  19.5 0.5 broadcast.2008
  20.0 0.6 reduce.3
  20.6 0.1 reshape.259
  20.7 4.2 %gather_fusion = bf16[64,64,512]{2,1,0:T(8,128)(2,1)} fusion(bf16[24,64,512]{2,1,0:T(8,128)(2,1)} %bitcast.21, s32[1024]{0:T(1024)S(1)} %pad_clamp_fusion), kind=kCustom, calls=%fused_computation | custom fusion | bytes 8388864 | tf_op jit(solution)/shard_map/gather | solution.py:146
  24.9 6.5 %all-to-all-start.1 = ((bf16[64,64,512]{2,1,0:T(8,128)(2,1)}), bf16[64,64,512]{2,1,0:T(8,128)(2,1)}, u32[]{:S(2)}, u32[]{:S(2)}) async-start(bf16[64,64,512]{2,1,0:T(8,128)(2,1)} %gather_fusion), calls=%async_computation.1 | async-start | bytes 8388608 | tf_op jit(solution)/shard_map/all_to_all | solution.py:148
  31.6 0.6 broadcast_multiply_fusion.scale_ref
  32.2 0.1 minimum_convert_fusion
  32.2 0.9 constant_dynamic-slice_fusion
  33.1 1.8 %collective-permute-start.3 = (bf16[256,1024]{1,0:T(8,128)(2,1)}, bf16[256,1024]{1,0:T(8,128)(2,1)}, u32[]{:S(2)}, u32[]{:S(2)}) collective-permute-start(bf16[256,1024]{1,0:T(8,128)(2,1)} %constant_dynamic-slice_fusion), channel_id=1, source_target_pairs={{0,1},{1,0},{2,3},{3,2},{4,5},{5,4},{6,7},{7,6},{8,9},{9,8},{10,11... | collective-permute-start | bytes 1572872 | tf_op jit(solution)/shard_map/ppermute | solution.py:50
  34.9 3.1 %fusion.3 = f32[1024]{0:T(1024)S(1)} fusion(bf16[1024,2048]{1,0:T(8,128)(2,1)} %param.14), kind=kLoop, calls=%fused_computation.8 | loop fusion | flops 6290432 | bytes 4198400 | tf_op jit(solution)/shard_map/reduce_sum | solution.py:18
  38.0 4.2 %convolution_convert_fusion.2 = bf16[1024,512]{0,1:T(8,128)(2,1)S(1)} fusion(bf16[2048,512]{1,0:T(8,128)(2,1)} %param.19, bf16[1024,2048]{1,0:T(8,128)(2,1)S(1)} %copy-done.2, f32[2048]{0:T(1024)S(1)} %copy-done.14, f32[1024]{0:T(1024)S(1)} %add_rsqrt_fusion.1), kind=kOutput, calls=%fused_computation.63 | convolution fusion | flops 2156396544 | bytes 7352320 | tf_op jit(solution)/shard_map/dot_general | solution.py:26
  42.2 0.0 copy-start.13
  42.2 1.6 %copy.75 = f32[1024,2,256]{2,0,1:T(8,128)} copy(bf16[1024,2,256]{0,2,1:T(8,128)(2,1)S(1)} %bitcast.23) | data formatting | bytes 3145728 | tf_op jit(solution)/shard_map/reshape | solution.py:27
  43.8 18.1 %convolution_convert_fusion.1 = bf16[2,1024,256]{1,2,0:T(8,128)(2,1)} fusion(bf16[2,256,256]{2,1,0:T(8,128)(2,1)S(1)} %copy-done.13, f32[1024,2,256]{2,0,1:T(8,128)} %copy.75, f32[1024,2]{0,1:T(2,128)S(1)} %minimum_convert_fusion, f32[2]{0:T(128)S(1)} %get-tuple-element.15, f32[2]{0:T(128)S(1)} %get-tuple-element.16, f32[2]{0:T(128)S(1)} %get-tuple-element.17, ...), kind=kOutput, calls=%fused_computation.62 | convolution fusion | flops 286785536 | bytes 3416192 | tf_op jit(solution)/shard_map/tgc,gcd->tgd/dot_general | solution.py:37
  61.9 0.4 collective-permute-start
  62.3 0.1 constant_dynamic-slice_fusion.1
  62.4 0.0 copy-start.3
  62.4 0.0 copy-start.12
  62.4 0.2 collective-permute-start.1
  62.7 4.0 %fusion.39 = bf16[1024,1024]{1,0:T(8,128)(2,1)} fusion(bf16[1024,512]{0,1:T(8,128)(2,1)} %bitcast.7, bf16[512,2048]{1,0:T(8,128)(2,1)S(1)} %copy-done, s32[]{:T(128)S(6)} %select_n.499), kind=kOutput, calls=%fused_computation.65 | convolution fusion | flops 1073741824 | bytes 4194308 | tf_op jit(solution)/shard_map/dot_general | solution.py:43
  66.7 2.1 %convolution_convert_fusion.3.q_ref = bf16[1024,256]{1,0:T(8,128)(2,1)} fusion(bf16[2048,256]{1,0:T(8,128)(2,1)S(1)} %copy-done.12, bf16[1024,2048]{1,0:T(8,128)(2,1)S(1)} %copy-done.3, f32[2048]{0:T(1024)S(1)} %copy-done.14, f32[1024]{0:T(1024)S(1)} %add_rsqrt_fusion.1), kind=kOutput, calls=%fused_computation.64 | convolution fusion | flops 1082392576 | bytes 5779456 | tf_op jit(solution)/shard_map/dot_general | solution.py:157
  68.8 0.1 copy-done.9
  68.8 6.3 %fusion.50 = f32[1024,1024]{1,0:T(8,128)} fusion(bf16[2048,1024]{1,0:T(8,128)(2,1)S(1)} %copy-done.9, bf16[1024,2048]{1,0:T(8,128)(2,1)S(1)} %copy-done.3, f32[2048]{0:T(1024)S(1)} %copy-done.14, f32[1024]{0:T(1024)S(1)} %add_rsqrt_fusion.1), kind=kOutput, calls=%fused_computation.113 | convolution fusion | flops 4303355904 | bytes 12595200 | tf_op jit(solution)/shard_map/dot_general | solution.py:156
  75.1 49.8 %all-to-all-done.1.refs_0_.refs_1_.refs_2_.refs_3_.refs_4_.refs_5_.refs_6_.refs_7_.refs_8_.refs_9_.refs_10_.refs_11_.refs_12_.refs_13_.refs_14_.refs_15_ = bf16[64,64,512]{2,1,0:T(8,128)(2,1)} async-done(((bf16[64,64,512]{2,1,0:T(8,128)(2,1)}), bf16[64,64,512]{2,1,0:T(8,128)(2,1)}, u32[]{:S(2)}, u32[]{:S(2)}) %all-to-all-start.1) | async-done | bytes 4194336 | tf_op jit(solution)/shard_map/all_to_all | solution.py:148
  125.0 5.5 %shard_map.136 = bf16[1024,256]{1,0:T(8,128)(2,1)} custom-call(s32[32]{0:T(128)} %copy-done.8, f32[2]{0:T(128)} %broadcast_multiply_fusion.scale_ref, bf16[1024,256]{1,0:T(8,128)(2,1)} %convolution_convert_fusion.3.q_ref, ...), custom_call_target="tpu_custom_call" | custom-call | flops 268435456 | bytes 4194304 | tf_op jit(solution)/shard_map/pallas_call | solution.py:92
  130.5 0.0 copy-start.6
  130.5 1.5 %collective-permute-start.2 = (bf16[1024,256]{1,0:T(8,128)(2,1)}, bf16[1024,256]{1,0:T(8,128)(2,1)S(1)}, u32[]{:S(2)}, u32[]{:S(2)}) collective-permute-start(bf16[1024,256]{1,0:T(8,128)(2,1)} %shard_map.136), channel_id=1, source_target_pairs={{0,1},{1,0},{2,3},{3,2},{4,5},{5,4},{6,7},{7,6},{8,9},{9,8},{10,11... | collective-permute-start | bytes 1572872 | tf_op jit(solution)/shard_map/ppermute | solution.py:50
  132.0 0.0 collective-permute-done
  132.0 0.0 collective-permute-done.1
  132.0 3.0 %fusion.53 = bf16[1024,1024]{1,0:T(8,128)(2,1)S(1)} fusion(bf16[1024,512]{0,1:T(8,128)(2,1)} %collective-permute-done, bf16[512,1024]{1,0:T(8,128)(2,1)} %collective-permute-done.1), kind=kOutput, calls=%fused_computation.114 | convolution fusion | flops 1073741824 | bytes 4194304 | tf_op jit(solution)/shard_map/dot_general | solution.py:43
  135.0 0.0 copy-start.16
  135.0 0.7 fusion.41
  135.7 0.0 collective-permute-done.3
  135.8 0.8 copy-done.16
  136.6 4.1 %add_convert_fusion = bf16[1024,1024]{1,0:T(8,128)(2,1)} fusion(f32[1024,1024]{1,0:T(8,128)S(1)} %copy-done.17, bf16[1024,1024]{1,0:T(8,128)(2,1)S(1)} %fusion.41, bf16[1024,1024]{1,0:T(8,128)(2,1)S(1)} %fusion.53, bf16[1024,1024]{1,0:T(8,128)(2,1)S(1)} %copy-done.16, bf16[1024,256]{1,0:T(8,128)(2,1)S(1)} %collective-permute-done.2, ...), kind=kOutput, calls=%fused_computation.11 | convolution fusion | flops 550502400 | bytes 13631488 | tf_op jit(solution)/shard_map/dot_general | solution.py:43
  (43 shorter events, 0.2 us)
Async XLA Ops:
  0.0 62.3 %copy-start = (bf16[512,2048]{1,0:T(8,128)(2,1)S(1)}, bf16[512,2048]{1,0:T(8,128)(2,1)}, u32[]{:S(2)}) copy-start(bf16[512,2048]{1,0:T(8,128)(2,1)} %param.21) | copy-start | bytes 6291460
  1.2 11.6 %copy-start.8 = (s32[32]{0:T(128)}, s32[32]{0:T(128)S(1)}, u32[]{:S(2)}) copy-start(s32[32]{0:T(128)S(1)} %multiply_add_fusion.slots_ref) | copy-start | bytes 388
  2.0 17.5 %all-to-all-start = ((s32[16,1,4]{2,1,0:T(1,128)}), s32[16,1,4]{2,1,0:T(1,128)S(1)}, u32[]{:S(2)}, u32[]{:S(2)}) async-start(s32[16,1,4]{2,1,0:T(1,128)} %bitcast.2), calls=%async_computation | async-start | bytes 16384 | tf_op jit(solution)/shard_map/all_to_all | solution.py:140
  8.6 4.6 %copy-start.1 = (bf16[24,64,2048]{2,1,0:T(8,128)(2,1)S(1)}, bf16[24,64,2048]{2,1,0:T(8,128)(2,1)}, u32[]{:S(2)}) copy-start(bf16[24,64,2048]{2,1,0:T(8,128)(2,1)} %param.16) | copy-start | bytes 18874372
  8.6 4.6 %copy-start.7 = (f32[2048]{0:T(1024)S(1)}, f32[2048]{0:T(1024)}, u32[]{:S(2)}) copy-start(f32[2048]{0:T(1024)} %param.17) | copy-start | bytes 24580
  13.2 1.5 %copy-start.10 = (bf16[2048,256]{1,0:T(8,128)(2,1)S(1)}, bf16[2048,256]{1,0:T(8,128)(2,1)}, u32[]{:S(2)}) copy-start(bf16[2048,256]{1,0:T(8,128)(2,1)} %param.24) | copy-start | bytes 3145732
  13.2 1.5 %copy-start.11 = (bf16[2048,256]{1,0:T(8,128)(2,1)S(1)}, bf16[2048,256]{1,0:T(8,128)(2,1)}, u32[]{:S(2)}) copy-start(bf16[2048,256]{1,0:T(8,128)(2,1)} %param.23) | copy-start | bytes 3145732
  24.9 6.7 %copy-start.15 = (f32[2]{0:T(128)S(1)}, f32[2]{0:T(128)}, u32[]{:S(2)}) copy-start(f32[2]{0:T(128)} %param.25) | copy-start | bytes 28
  24.9 7.3 %copy-start.5 = (bf16[256,2048]{1,0:T(8,128)(2,1)S(1)}, bf16[256,2048]{1,0:T(8,128)(2,1)}, u32[]{:S(2)}) copy-start(bf16[256,2048]{1,0:T(8,128)(2,1)} %param.26) | copy-start | bytes 3145732
  24.9 100.0 %all-to-all-start.1 = ((bf16[64,64,512]{2,1,0:T(8,128)(2,1)}), bf16[64,64,512]{2,1,0:T(8,128)(2,1)}, u32[]{:S(2)}, u32[]{:S(2)}) async-start(bf16[64,64,512]{2,1,0:T(8,128)(2,1)} %gather_fusion), calls=%async_computation.1 | async-start | bytes 8388608 | tf_op jit(solution)/shard_map/all_to_all | solution.py:148
  33.1 4.9 %copy-start.2 = (bf16[1024,2048]{1,0:T(8,128)(2,1)S(1)}, bf16[1024,2048]{1,0:T(8,128)(2,1)}, u32[]{:S(2)}) copy-start(bf16[1024,2048]{1,0:T(8,128)(2,1)} %param.14) | copy-start | bytes 12582916
  33.1 4.9 %copy-start.14 = (f32[2048]{0:T(1024)S(1)}, f32[2048]{0:T(1024)}, u32[]{:S(2)}) copy-start(f32[2048]{0:T(1024)} %param.15) | copy-start | bytes 24580
  33.1 102.6 %collective-permute-start.3 = (bf16[256,1024]{1,0:T(8,128)(2,1)}, bf16[256,1024]{1,0:T(8,128)(2,1)}, u32[]{:S(2)}, u32[]{:S(2)}) collective-permute-start(bf16[256,1024]{1,0:T(8,128)(2,1)} %constant_dynamic-slice_fusion), channel_id=1, source_target_pairs={{0,1},{1,0},{2,3},{3,2},{4,5},{5,4},{6,7},{7,6},{8,9},{9,8},{10,11... | collective-permute-start | bytes 1572872 | tf_op jit(solution)/shard_map/ppermute | solution.py:50
  42.2 1.6 %copy-start.13 = (bf16[2,256,256]{2,1,0:T(8,128)(2,1)S(1)}, bf16[2,256,256]{2,1,0:T(8,128)(2,1)}, u32[]{:S(2)}) copy-start(bf16[2,256,256]{2,1,0:T(8,128)(2,1)} %param.20) | copy-start | bytes 786436
  61.9 70.1 %collective-permute-start = (bf16[1024,512]{0,1:T(8,128)(2,1)}, bf16[1024,512]{0,1:T(8,128)(2,1)}, u32[]{:S(2)}, u32[]{:S(2)}) collective-permute-start(bf16[1024,512]{0,1:T(8,128)(2,1)} %bitcast.7), channel_id=1, source_target_pairs={{0,1},{1,0},{2,3},{3,2},{4,5},{5,4},{6,7},{7,6},{8,9},{9,8},{10,11... | collective-permute-start | bytes 3145736 | tf_op jit(solution)/shard_map/ppermute | solution.py:50
  62.4 4.3 %copy-start.3 = (bf16[1024,2048]{1,0:T(8,128)(2,1)S(1)}, bf16[1024,2048]{1,0:T(8,128)(2,1)}, u32[]{:S(2)}) copy-start(bf16[1024,2048]{1,0:T(8,128)(2,1)} %param.14) | copy-start | bytes 12582916
  62.4 4.2 %copy-start.12 = (bf16[2048,256]{1,0:T(8,128)(2,1)S(1)}, bf16[2048,256]{1,0:T(8,128)(2,1)}, u32[]{:S(2)}) copy-start(bf16[2048,256]{1,0:T(8,128)(2,1)} %param.22) | copy-start | bytes 3145732
  62.4 69.6 %collective-permute-start.1 = (bf16[512,1024]{1,0:T(8,128)(2,1)S(1)}, bf16[512,1024]{1,0:T(8,128)(2,1)}, u32[]{:S(2)}, u32[]{:S(2)}) collective-permute-start(bf16[512,1024]{1,0:T(8,128)(2,1)S(1)} %constant_dynamic-slice_fusion.1), channel_id=1, source_target_pairs={{0,1},{1,0},{2,3},{3,2},{4,5},{5,4},{6,7},{7,6},{8,9},{9,8},{10,11... | collective-permute-start | bytes 3145736 | tf_op jit(solution)/shard_map/ppermute | solution.py:50
  66.6 2.2 %copy-start.9 = (bf16[2048,1024]{1,0:T(8,128)(2,1)S(1)}, bf16[2048,1024]{1,0:T(8,128)(2,1)}, u32[]{:S(2)}) copy-start(bf16[2048,1024]{1,0:T(8,128)(2,1)} %param.27) | copy-start | bytes 12582916
  130.5 4.5 %copy-start.4 = (bf16[1024,256]{1,0:T(8,128)(2,1)S(1)}, bf16[1024,256]{1,0:T(8,128)(2,1)}, u32[]{:S(2)}) copy-start(bf16[1024,256]{1,0:T(8,128)(2,1)} %shard_map.136) | copy-start | bytes 1572868
  130.5 4.5 %copy-start.6 = (bf16[256,2048]{1,0:T(8,128)(2,1)S(1)}, bf16[256,2048]{1,0:T(8,128)(2,1)}, u32[]{:S(2)}) copy-start(bf16[256,2048]{1,0:T(8,128)(2,1)} %param.26) | copy-start | bytes 3145732
  130.5 5.2 %collective-permute-start.2 = (bf16[1024,256]{1,0:T(8,128)(2,1)}, bf16[1024,256]{1,0:T(8,128)(2,1)S(1)}, u32[]{:S(2)}, u32[]{:S(2)}) collective-permute-start(bf16[1024,256]{1,0:T(8,128)(2,1)} %shard_map.136), channel_id=1, source_target_pairs={{0,1},{1,0},{2,3},{3,2},{4,5},{5,4},{6,7},{7,6},{8,9},{9,8},{10,11... | collective-permute-start | bytes 1572872 | tf_op jit(solution)/shard_map/ppermute | solution.py:50
  132.0 3.8 %copy-start.17 = (f32[1024,1024]{1,0:T(8,128)S(1)}, f32[1024,1024]{1,0:T(8,128)}, u32[]{:S(2)}) copy-start(f32[1024,1024]{1,0:T(8,128)} %fusion.50) | copy-start | bytes 12582916
  135.0 1.6 %copy-start.16 = (bf16[1024,1024]{1,0:T(8,128)(2,1)S(1)}, bf16[1024,1024]{1,0:T(8,128)(2,1)}, u32[]{:S(2)}) copy-start(bf16[1024,1024]{1,0:T(8,128)(2,1)} %fusion.39) | copy-start | bytes 6291460

commit v3 on v2

--- a/solution.py
+++ b/solution.py
@@ -9,7 +9,7 @@
 from jax.sharding import PartitionSpec as P
 
 GROUPS = 4
-ATTEND_BLOCKS = 4
+ATTEND_BLOCKS = 8
 MESH = pl.DeviceIdType.MESH
 
 

time: 141 us -> 140 us (level)
  transfers between devices with their start and end apart: 6 -> 6, of which waited for: 1 -> 1; matrix products, arithmetic and copies ran while one was open for 39% -> 39% of each run, Pallas kernels for 4% -> 3%
where the time goes in v3:
time: 140 us
  waiting for transfers between devices  49.9 us (36%)
  matrix products  47.2 us (34%)
  starting transfers between devices  17 us (12%)
  other arithmetic  10.5 us (8%)
  local copies, waits for them, and re-layouts  10.4 us (7%)
  Pallas kernels  4.83 us (3%)
    all_to_all x1, waiting for transfers between devices, body(): kv = lax.all_to_all(packed, 'st', split_axis=0, concat_axis=0, tiled=True)  49.8 us
    dot_general x1, matrix products, pool_branch(): jnp.einsum('tgc,gcd->tgd', pooled, pool_mix, preferred_element_type=jnp.f...  18.1 us
    dot_general x4, matrix products, half_terms(): jnp.dot(a, w, preferred_element_type=jnp.float32).astype(jnp.bfloat16)  11.8 us
    reduce_sum x2, other arithmetic, rms_norm(): scale = lax.rsqrt(jnp.mean(wide * wide, axis=-1, keepdims=True) + 1e-05)  7.3 us
    all_to_all x1, starting transfers between devices, body(): lax.all_to_all(request, 'st', split_axis=0, concat_axis=0, tiled=True)  6.58 us
    all_to_all x1, starting transfers between devices, body(): kv = lax.all_to_all(packed, 'st', split_axis=0, concat_axis=0, tiled=True)  6.49 us
    dot_general x1, matrix products, body(): jnp.dot(normed, w_gate, preferred_element_type=jnp.float32)  6.27 us
    pallas_call x1, Pallas kernels, attend(): pl.pallas_call(functools.partial(attention_kernel, heads, group), out_sha...  4.83 us
  transfers between devices with their start and end apart: 6, of which 1 were waited for; matrix products, arithmetic and copies ran while one was open for 39% of the time, Pallas kernels for 3%

profile of v3, /device:TPU:15, one launch (start us, length us, event | category | flops | bytes accessed | tf_op | source)
XLA Modules:
  0.0 140.0 jit_solution(13067067701625103407)
XLA Ops:
  0.0 0.9 copy.73
  0.9 0.1 reshape.258
  1.0 0.2 convert_reduce_fusion
  1.2 0.1 select_reduce_fusion
  1.3 0.7 all_to_all.9
  2.0 6.6 %all-to-all-start = ((s32[16,1,4]{2,1,0:T(1,128)}), s32[16,1,4]{2,1,0:T(1,128)S(1)}, u32[]{:S(2)}, u32[]{:S(2)}) async-start(s32[16,1,4]{2,1,0:T(1,128)} %bitcast.2), calls=%async_computation | async-start | bytes 16384 | tf_op jit(solution)/shard_map/all_to_all | solution.py:140
  8.6 0.0 copy-start.7
  8.6 4.2 %fusion = f32[24,64]{1,0:T(8,128)S(1)} fusion(bf16[24,64,2048]{2,1,0:T(8,128)(2,1)} %param.16), kind=kLoop, calls=%fused_computation.3 | loop fusion | flops 9435648 | bytes 6297600 | tf_op jit(solution)/shard_map/reduce_sum | solution.py:18
  12.8 0.3 copy-done.1
  13.2 1.5 %fusion.2 = bf16[24,64,2048]{2,1,0:T(8,128)(2,1)S(1)} fusion(bf16[24,64,2048]{2,1,0:T(8,128)(2,1)S(1)} %copy-done.1, f32[2048]{0:T(1024)S(1)} %copy-done.7, f32[24,64]{1,0:T(8,128)S(1)} %add_rsqrt_fusion), kind=kLoop, calls=%fused_computation.5 | loop fusion | flops 12582912 | bytes 12597248 | tf_op jit(solution)/shard_map/convert_element_type | solution.py:142
  14.7 0.0 copy-done.11
  14.7 4.8 %convolution_convert_fusion = bf16[1536,512]{1,0:T(8,128)(2,1)} fusion(bf16[1536,2048]{1,0:T(8,128)(2,1)S(1)} %bitcast.22, bf16[2048,256]{1,0:T(8,128)(2,1)S(1)} %copy-done.10, bf16[2048,256]{1,0:T(8,128)(2,1)S(1)} %copy-done.11), kind=kOutput, calls=%fused_computation.12 | convolution fusion | flops 3226206208 | bytes 9961472 | tf_op jit(solution)/shard_map/dot_general | solution.py:144
  19.5 0.0 all-to-all-done
  19.5 0.5 broadcast.2008
  20.0 0.6 reduce.3
  20.6 0.1 reshape.259
  20.7 4.2 %gather_fusion = bf16[64,64,512]{2,1,0:T(8,128)(2,1)} fusion(bf16[24,64,512]{2,1,0:T(8,128)(2,1)} %bitcast.21, s32[1024]{0:T(1024)S(1)} %pad_clamp_fusion), kind=kCustom, calls=%fused_computation | custom fusion | bytes 8388864 | tf_op jit(solution)/shard_map/gather | solution.py:146
  24.9 6.5 %all-to-all-start.1 = ((bf16[64,64,512]{2,1,0:T(8,128)(2,1)}), bf16[64,64,512]{2,1,0:T(8,128)(2,1)}, u32[]{:S(2)}, u32[]{:S(2)}) async-start(bf16[64,64,512]{2,1,0:T(8,128)(2,1)} %gather_fusion), calls=%async_computation.1 | async-start | bytes 8388608 | tf_op jit(solution)/shard_map/all_to_all | solution.py:148
  31.6 0.6 broadcast_multiply_fusion.scale_ref
  32.2 0.1 minimum_convert_fusion
  32.2 0.9 constant_dynamic-slice_fusion
  33.1 1.8 %collective-permute-start.3 = (bf16[256,1024]{1,0:T(8,128)(2,1)}, bf16[256,1024]{1,0:T(8,128)(2,1)}, u32[]{:S(2)}, u32[]{:S(2)}) collective-permute-start(bf16[256,1024]{1,0:T(8,128)(2,1)} %constant_dynamic-slice_fusion), channel_id=1, source_target_pairs={{0,1},{1,0},{2,3},{3,2},{4,5},{5,4},{6,7},{7,6},{8,9},{9,8},{10,11... | collective-permute-start | bytes 1572872 | tf_op jit(solution)/shard_map/ppermute | solution.py:50
  34.9 3.1 %fusion.3 = f32[1024]{0:T(1024)S(1)} fusion(bf16[1024,2048]{1,0:T(8,128)(2,1)} %param.14), kind=kLoop, calls=%fused_computation.8 | loop fusion | flops 6290432 | bytes 4198400 | tf_op jit(solution)/shard_map/reduce_sum | solution.py:18
  38.0 4.2 %convolution_convert_fusion.2 = bf16[1024,512]{0,1:T(8,128)(2,1)S(1)} fusion(bf16[2048,512]{1,0:T(8,128)(2,1)} %param.19, bf16[1024,2048]{1,0:T(8,128)(2,1)S(1)} %copy-done.2, f32[2048]{0:T(1024)S(1)} %copy-done.14, f32[1024]{0:T(1024)S(1)} %add_rsqrt_fusion.1), kind=kOutput, calls=%fused_computation.63 | convolution fusion | flops 2156396544 | bytes 7352320 | tf_op jit(solution)/shard_map/dot_general | solution.py:26
  42.2 0.0 copy-start.13
  42.2 1.6 %copy.75 = f32[1024,2,256]{2,0,1:T(8,128)} copy(bf16[1024,2,256]{0,2,1:T(8,128)(2,1)S(1)} %bitcast.23) | data formatting | bytes 3145728 | tf_op jit(solution)/shard_map/reshape | solution.py:27
  43.8 18.1 %convolution_convert_fusion.1 = bf16[2,1024,256]{1,2,0:T(8,128)(2,1)} fusion(bf16[2,256,256]{2,1,0:T(8,128)(2,1)S(1)} %copy-done.13, f32[1024,2,256]{2,0,1:T(8,128)} %copy.75, f32[1024,2]{0,1:T(2,128)S(1)} %minimum_convert_fusion, f32[2]{0:T(128)S(1)} %get-tuple-element.15, f32[2]{0:T(128)S(1)} %get-tuple-element.16, f32[2]{0:T(128)S(1)} %get-tuple-element.17, ...), kind=kOutput, calls=%fused_computation.62 | convolution fusion | flops 286785536 | bytes 3416192 | tf_op jit(solution)/shard_map/tgc,gcd->tgd/dot_general | solution.py:37
  61.9 0.4 collective-permute-start
  62.3 0.1 constant_dynamic-slice_fusion.1
  62.4 0.0 copy-start.3
  62.4 0.0 copy-start.12
  62.4 0.2 collective-permute-start.1
  62.7 4.0 %fusion.39 = bf16[1024,1024]{1,0:T(8,128)(2,1)} fusion(bf16[1024,512]{0,1:T(8,128)(2,1)} %bitcast.7, bf16[512,2048]{1,0:T(8,128)(2,1)S(1)} %copy-done, s32[]{:T(128)S(6)} %select_n.499), kind=kOutput, calls=%fused_computation.65 | convolution fusion | flops 1073741824 | bytes 4194308 | tf_op jit(solution)/shard_map/dot_general | solution.py:43
  66.7 2.1 %convolution_convert_fusion.3.q_ref = bf16[1024,256]{1,0:T(8,128)(2,1)} fusion(bf16[2048,256]{1,0:T(8,128)(2,1)S(1)} %copy-done.12, bf16[1024,2048]{1,0:T(8,128)(2,1)S(1)} %copy-done.3, f32[2048]{0:T(1024)S(1)} %copy-done.14, f32[1024]{0:T(1024)S(1)} %add_rsqrt_fusion.1), kind=kOutput, calls=%fused_computation.64 | convolution fusion | flops 1082392576 | bytes 5779456 | tf_op jit(solution)/shard_map/dot_general | solution.py:157
  68.8 0.1 copy-done.9
  68.8 6.3 %fusion.50 = f32[1024,1024]{1,0:T(8,128)} fusion(bf16[2048,1024]{1,0:T(8,128)(2,1)S(1)} %copy-done.9, bf16[1024,2048]{1,0:T(8,128)(2,1)S(1)} %copy-done.3, f32[2048]{0:T(1024)S(1)} %copy-done.14, f32[1024]{0:T(1024)S(1)} %add_rsqrt_fusion.1), kind=kOutput, calls=%fused_computation.113 | convolution fusion | flops 4303355904 | bytes 12595200 | tf_op jit(solution)/shard_map/dot_general | solution.py:156
  75.1 49.8 %all-to-all-done.1.refs_0_.refs_1_.refs_2_.refs_3_.refs_4_.refs_5_.refs_6_.refs_7_.refs_8_.refs_9_.refs_10_.refs_11_.refs_12_.refs_13_.refs_14_.refs_15_.refs_16_.refs_17_.refs_18_.refs_19_.refs_20_.refs_21_.refs_22_.refs_23_.refs_24_.refs_25_.refs_26_.refs_27_.refs_28_.refs_29_.refs_30_.refs_31_ = bf16[64,64,512]{2,1,0:T(8,128)(2,1)} async-done(((bf16[64,64,512]{2,1,0:T(8,128)(2,1)}), ...) | async-done | bytes 4194336 | tf_op jit(solution)/shard_map/all_to_all | solution.py:148
  125.0 4.8 %shard_map.136 = bf16[1024,256]{1,0:T(8,128)(2,1)} custom-call(s32[32]{0:T(128)} %copy-done.8, f32[2]{0:T(128)} %broadcast_multiply_fusion.scale_ref, bf16[1024,256]{1,0:T(8,128)(2,1)} %convolution_convert_fusion.3.q_ref, ...), custom_call_target="tpu_custom_call" | custom-call | flops 268435456 | bytes 4194304 | tf_op jit(solution)/shard_map/pallas_call | solution.py:92
  129.8 0.0 copy-start.6
  129.8 1.5 %collective-permute-start.2 = (bf16[1024,256]{1,0:T(8,128)(2,1)}, bf16[1024,256]{1,0:T(8,128)(2,1)S(1)}, u32[]{:S(2)}, u32[]{:S(2)}) collective-permute-start(bf16[1024,256]{1,0:T(8,128)(2,1)} %shard_map.136), channel_id=1, source_target_pairs={{0,1},{1,0},{2,3},{3,2},{4,5},{5,4},{6,7},{7,6},{8,9},{9,8},{10,11... | collective-permute-start | bytes 1572872 | tf_op jit(solution)/shard_map/ppermute | solution.py:50
  131.3 0.0 collective-permute-done
  131.3 0.0 collective-permute-done.1
  131.3 3.0 %fusion.53 = bf16[1024,1024]{1,0:T(8,128)(2,1)S(1)} fusion(bf16[1024,512]{0,1:T(8,128)(2,1)} %collective-permute-done, bf16[512,1024]{1,0:T(8,128)(2,1)} %collective-permute-done.1), kind=kOutput, calls=%fused_computation.114 | convolution fusion | flops 1073741824 | bytes 4194304 | tf_op jit(solution)/shard_map/dot_general | solution.py:43
  134.3 0.0 copy-start.16
  134.3 0.7 fusion.41
  135.0 0.0 collective-permute-done.2
  135.1 0.8 copy-done.16
  135.9 4.1 %add_convert_fusion = bf16[1024,1024]{1,0:T(8,128)(2,1)} fusion(f32[1024,1024]{1,0:T(8,128)S(1)} %copy-done.17, bf16[1024,1024]{1,0:T(8,128)(2,1)S(1)} %fusion.41, bf16[1024,1024]{1,0:T(8,128)(2,1)S(1)} %fusion.53, bf16[1024,1024]{1,0:T(8,128)(2,1)S(1)} %copy-done.16, bf16[1024,256]{1,0:T(8,128)(2,1)S(1)} %collective-permute-done.2, ...), kind=kOutput, calls=%fused_computation.11 | convolution fusion | flops 550502400 | bytes 13631488 | tf_op jit(solution)/shard_map/dot_general | solution.py:43
  (43 shorter events, 0.2 us)
Async XLA Ops:
  0.0 62.3 %copy-start = (bf16[512,2048]{1,0:T(8,128)(2,1)S(1)}, bf16[512,2048]{1,0:T(8,128)(2,1)}, u32[]{:S(2)}) copy-start(bf16[512,2048]{1,0:T(8,128)(2,1)} %param.21) | copy-start | bytes 6291460
  1.2 11.6 %copy-start.8 = (s32[32]{0:T(128)}, s32[32]{0:T(128)S(1)}, u32[]{:S(2)}) copy-start(s32[32]{0:T(128)S(1)} %multiply_add_fusion.slots_ref) | copy-start | bytes 388
  2.0 17.5 %all-to-all-start = ((s32[16,1,4]{2,1,0:T(1,128)}), s32[16,1,4]{2,1,0:T(1,128)S(1)}, u32[]{:S(2)}, u32[]{:S(2)}) async-start(s32[16,1,4]{2,1,0:T(1,128)} %bitcast.2), calls=%async_computation | async-start | bytes 16384 | tf_op jit(solution)/shard_map/all_to_all | solution.py:140
  8.6 4.6 %copy-start.1 = (bf16[24,64,2048]{2,1,0:T(8,128)(2,1)S(1)}, bf16[24,64,2048]{2,1,0:T(8,128)(2,1)}, u32[]{:S(2)}) copy-start(bf16[24,64,2048]{2,1,0:T(8,128)(2,1)} %param.16) | copy-start | bytes 18874372
  8.6 4.6 %copy-start.7 = (f32[2048]{0:T(1024)S(1)}, f32[2048]{0:T(1024)}, u32[]{:S(2)}) copy-start(f32[2048]{0:T(1024)} %param.17) | copy-start | bytes 24580
  13.2 1.5 %copy-start.10 = (bf16[2048,256]{1,0:T(8,128)(2,1)S(1)}, bf16[2048,256]{1,0:T(8,128)(2,1)}, u32[]{:S(2)}) copy-start(bf16[2048,256]{1,0:T(8,128)(2,1)} %param.24) | copy-start | bytes 3145732
  13.2 1.5 %copy-start.11 = (bf16[2048,256]{1,0:T(8,128)(2,1)S(1)}, bf16[2048,256]{1,0:T(8,128)(2,1)}, u32[]{:S(2)}) copy-start(bf16[2048,256]{1,0:T(8,128)(2,1)} %param.23) | copy-start | bytes 3145732
  24.9 6.7 %copy-start.15 = (f32[2]{0:T(128)S(1)}, f32[2]{0:T(128)}, u32[]{:S(2)}) copy-start(f32[2]{0:T(128)} %param.25) | copy-start | bytes 28
  24.9 7.3 %copy-start.5 = (bf16[256,2048]{1,0:T(8,128)(2,1)S(1)}, bf16[256,2048]{1,0:T(8,128)(2,1)}, u32[]{:S(2)}) copy-start(bf16[256,2048]{1,0:T(8,128)(2,1)} %param.26) | copy-start | bytes 3145732
  24.9 100.0 %all-to-all-start.1 = ((bf16[64,64,512]{2,1,0:T(8,128)(2,1)}), bf16[64,64,512]{2,1,0:T(8,128)(2,1)}, u32[]{:S(2)}, u32[]{:S(2)}) async-start(bf16[64,64,512]{2,1,0:T(8,128)(2,1)} %gather_fusion), calls=%async_computation.1 | async-start | bytes 8388608 | tf_op jit(solution)/shard_map/all_to_all | solution.py:148
  33.1 4.9 %copy-start.2 = (bf16[1024,2048]{1,0:T(8,128)(2,1)S(1)}, bf16[1024,2048]{1,0:T(8,128)(2,1)}, u32[]{:S(2)}) copy-start(bf16[1024,2048]{1,0:T(8,128)(2,1)} %param.14) | copy-start | bytes 12582916
  33.1 4.9 %copy-start.14 = (f32[2048]{0:T(1024)S(1)}, f32[2048]{0:T(1024)}, u32[]{:S(2)}) copy-start(f32[2048]{0:T(1024)} %param.15) | copy-start | bytes 24580
  33.1 101.9 %collective-permute-start.3 = (bf16[256,1024]{1,0:T(8,128)(2,1)}, bf16[256,1024]{1,0:T(8,128)(2,1)}, u32[]{:S(2)}, u32[]{:S(2)}) collective-permute-start(bf16[256,1024]{1,0:T(8,128)(2,1)} %constant_dynamic-slice_fusion), channel_id=1, source_target_pairs={{0,1},{1,0},{2,3},{3,2},{4,5},{5,4},{6,7},{7,6},{8,9},{9,8},{10,11... | collective-permute-start | bytes 1572872 | tf_op jit(solution)/shard_map/ppermute | solution.py:50
  42.2 1.6 %copy-start.13 = (bf16[2,256,256]{2,1,0:T(8,128)(2,1)S(1)}, bf16[2,256,256]{2,1,0:T(8,128)(2,1)}, u32[]{:S(2)}) copy-start(bf16[2,256,256]{2,1,0:T(8,128)(2,1)} %param.20) | copy-start | bytes 786436
  61.9 69.4 %collective-permute-start = (bf16[1024,512]{0,1:T(8,128)(2,1)}, bf16[1024,512]{0,1:T(8,128)(2,1)}, u32[]{:S(2)}, u32[]{:S(2)}) collective-permute-start(bf16[1024,512]{0,1:T(8,128)(2,1)} %bitcast.7), channel_id=1, source_target_pairs={{0,1},{1,0},{2,3},{3,2},{4,5},{5,4},{6,7},{7,6},{8,9},{9,8},{10,11... | collective-permute-start | bytes 3145736 | tf_op jit(solution)/shard_map/ppermute | solution.py:50
  62.4 4.3 %copy-start.3 = (bf16[1024,2048]{1,0:T(8,128)(2,1)S(1)}, bf16[1024,2048]{1,0:T(8,128)(2,1)}, u32[]{:S(2)}) copy-start(bf16[1024,2048]{1,0:T(8,128)(2,1)} %param.14) | copy-start | bytes 12582916
  62.4 4.2 %copy-start.12 = (bf16[2048,256]{1,0:T(8,128)(2,1)S(1)}, bf16[2048,256]{1,0:T(8,128)(2,1)}, u32[]{:S(2)}) copy-start(bf16[2048,256]{1,0:T(8,128)(2,1)} %param.22) | copy-start | bytes 3145732
  62.4 68.9 %collective-permute-start.1 = (bf16[512,1024]{1,0:T(8,128)(2,1)S(1)}, bf16[512,1024]{1,0:T(8,128)(2,1)}, u32[]{:S(2)}, u32[]{:S(2)}) collective-permute-start(bf16[512,1024]{1,0:T(8,128)(2,1)S(1)} %constant_dynamic-slice_fusion.1), channel_id=1, source_target_pairs={{0,1},{1,0},{2,3},{3,2},{4,5},{5,4},{6,7},{7,6},{8,9},{9,8},{10,11... | collective-permute-start | bytes 3145736 | tf_op jit(solution)/shard_map/ppermute | solution.py:50
  66.6 2.2 %copy-start.9 = (bf16[2048,1024]{1,0:T(8,128)(2,1)S(1)}, bf16[2048,1024]{1,0:T(8,128)(2,1)}, u32[]{:S(2)}) copy-start(bf16[2048,1024]{1,0:T(8,128)(2,1)} %param.27) | copy-start | bytes 12582916
  129.8 4.5 %copy-start.4 = (bf16[1024,256]{1,0:T(8,128)(2,1)S(1)}, bf16[1024,256]{1,0:T(8,128)(2,1)}, u32[]{:S(2)}) copy-start(bf16[1024,256]{1,0:T(8,128)(2,1)} %shard_map.136) | copy-start | bytes 1572868
  129.8 4.5 %copy-start.6 = (bf16[256,2048]{1,0:T(8,128)(2,1)S(1)}, bf16[256,2048]{1,0:T(8,128)(2,1)}, u32[]{:S(2)}) copy-start(bf16[256,2048]{1,0:T(8,128)(2,1)} %param.26) | copy-start | bytes 3145732
  129.8 5.2 %collective-permute-start.2 = (bf16[1024,256]{1,0:T(8,128)(2,1)}, bf16[1024,256]{1,0:T(8,128)(2,1)S(1)}, u32[]{:S(2)}, u32[]{:S(2)}) collective-permute-start(bf16[1024,256]{1,0:T(8,128)(2,1)} %shard_map.136), channel_id=1, source_target_pairs={{0,1},{1,0},{2,3},{3,2},{4,5},{5,4},{6,7},{7,6},{8,9},{9,8},{10,11... | collective-permute-start | bytes 1572872 | tf_op jit(solution)/shard_map/ppermute | solution.py:50
  131.3 3.8 %copy-start.17 = (f32[1024,1024]{1,0:T(8,128)S(1)}, f32[1024,1024]{1,0:T(8,128)}, u32[]{:S(2)}) copy-start(f32[1024,1024]{1,0:T(8,128)} %fusion.50) | copy-start | bytes 12582916
  134.3 1.6 %copy-start.16 = (bf16[1024,1024]{1,0:T(8,128)(2,1)S(1)}, bf16[1024,1024]{1,0:T(8,128)(2,1)}, u32[]{:S(2)}) copy-start(bf16[1024,1024]{1,0:T(8,128)(2,1)} %fusion.39) | copy-start | bytes 6291460
